TPU v7x, 128 devices: a whole 4x4x4 slice. The times are simulated.
128 devices in a mesh: sp: 16 (over z, y), dp: 8 (over x, core).
Axes of the slice: x: 4, y: 4, z: 4, core: 2. Of those that a mesh axis runs over, the one named last changes fastest.
Arguments:
- residual_input: bfloat16 [8, 2048, 2048], P('dp', 'sp'), may hold values from -6 to 6
- queries: bfloat16 [8, 2048, 1024], P('dp', 'sp'), may hold values from -6 to 6
- keys: bfloat16 [8, 2048, 1024], P('dp', 'sp'), may hold values from -6 to 6
- values: bfloat16 [8, 2048, 2048], P('dp', 'sp'), may hold values from -6 to 6
- gate_logits: bfloat16 [8, 2048, 64], P('dp', 'sp'), may hold values from -6 to 6
- retention_offset: float32 [16, 2], P('sp'), may hold values from 3 to 12
- log_forget_extra: float32 [8, 16, 2048], P('dp', 'sp'), may hold values from -2.76 to 0
- lane_amplifier: float32 [2048], P('sp'), may hold values from 0.1 to 1.9
- output_gate_logits: bfloat16 [8, 2048, 2048], P('dp', 'sp'), may hold values from -6 to 6
- output_projection: bfloat16 [2048, 2048], P(None, 'dp'), may hold values from -0.125 to 0.125
- cell_norm_gain: float32 [2048], replicated, may hold values from 0.1 to 1.9
- expert_norm_gain: float32 [2048], replicated, may hold values from 0.1 to 1.9
- expert_index: int32 [8, 2048, 2], P('dp', 'sp'), may hold values from 0 to 127, all different within a row; in each aligned block of 128 rows (0 to 127, 128 to 255, ..., all dimensions but the last counted through in order) at most 4 rows name the same one
- group_mixing_weight: float32 [8, 2048, 4], P('dp', 'sp'), may hold values from 0.05 to 1
- within_group_weight: float32 [8, 2048, 2], P('dp', 'sp'), may hold values from 0.1 to 1
- gate_weight: bfloat16 [128, 2048, 1024], P(('sp', 'dp')), may hold values from -0.125 to 0.125
- up_weight: bfloat16 [128, 2048, 1024], P(('sp', 'dp')), may hold values from -0.125 to 0.125
- down_weight: bfloat16 [128, 1024, 2048], P(('sp', 'dp')), may hold values from -0.75 to 0.75
Outputs:
- stream_out: bfloat16 [8, 2048, 2048], P('dp', 'sp')
Inputs may be any that keep to these rules, and one draw needn't show every extreme that they name: `expert_index`: A token's two experts differ; among the 128 tokens of one device no expert is named more than 4 times, a bound that some block reaches.
All inputs are finite; a program needn't handle non-finite values.
Results may differ from a plain program's by a relative error of at most 0.0095.
Values may be sent and summed in bfloat16 or wider, within the bound.
A program may use at most 128 MiB of HBM per device.

v0:
```python
from functools import partial

import jax
import jax.numpy as jnp
from jax import lax
from jax.experimental import pallas as pl
from jax.experimental.pallas import tpu as pltpu
from jax.sharding import PartitionSpec as P

EPS = 1e-06
HIGH = lax.Precision.HIGHEST
F32 = jnp.float32
BF16 = jnp.bfloat16
H = 16
DK = 64
DV = 128
C = 128
PAIRS = H // 2
NT = (((1,), (1,)), ((), ()))
TN = (((0,), (0,)), ((), ()))


def log_sigmoid(x):
    return jnp.minimum(x, 0.0) - jnp.log1p(jnp.exp(-jnp.abs(x)))


def cell_kernel(
    q_ref, k_ref, v_ref, g_ref, msg_ref, ogl_ref,
    out_ref,
    rx1, lst, lsm, rxs, rxm, ent, enm, est, esm,
    fcol, bcol, rows, nfb, zfb, sg,
    sa, ra, sb, rb, sc, rc, sd, rd, se, re,
):
    me = lax.axis_index("sp")

    def peer_of(d):
        return lax.rem(me + d, H)

    def remote(src, dst, ssem, rsem, peer):
        return pltpu.make_async_remote_copy(
            src_ref=src, dst_ref=dst, send_sem=ssem, recv_sem=rsem,
            device_id={"sp": peer}, device_id_type=pl.DeviceIdType.MESH,
        )

    def each_peer(body):
        def step(d, carry):
            body(peer_of(d))
            return carry

        lax.fori_loop(1, H, step, 0)

    barrier = pltpu.get_barrier_semaphore()
    each_peer(lambda p: pl.semaphore_signal(
        barrier, inc=1, device_id={"sp": p}, device_id_type=pl.DeviceIdType.MESH))
    pl.semaphore_wait(barrier, H - 1)

    each_peer(lambda p: remote(msg_ref.at[p], rx1.at[me], sa.at[p], ra.at[me], p).start())
    rx1[me] = msg_ref[me]

    lane = lax.broadcasted_iota(jnp.int32, (C, C), 1)
    low_half = lane < DK
    row_id = lax.broadcasted_iota(jnp.int32, (C, C), 0)
    earlier = lane <= row_id
    diagonal = lane == row_id

    def gate_step(p, carry):
        cols = pl.ds(pl.multiple_of(p * 256, 256), 256)
        sg[:, cols] = 1.0 / (1.0 + jnp.exp(-ogl_ref[:, cols].astype(F32)))
        return carry

    lax.fori_loop(0, PAIRS, gate_step, 0)

    each_peer(lambda p: remote(msg_ref.at[p], rx1.at[p], sa.at[p], ra.at[p], p).wait_recv())

    spread = rx1[:, 0, :]
    in_f = g_ref[0]
    in_b = g_ref[2]
    fade_f = log_sigmoid(g_ref[1] + rx1[:, 2, :]) + spread
    fade_b = log_sigmoid(g_ref[3] + rx1[:, 3, :]) + spread
    upto = (row_id <= lane).astype(F32)
    since = (row_id >= lane).astype(F32)
    cum_f = lax.dot_general(fade_f, upto, (((1,), (0,)), ((), ())), precision=HIGH, preferred_element_type=F32)
    cum_b = lax.dot_general(fade_b, since, (((1,), (0,)), ((), ())), precision=HIGH, preferred_element_type=F32)
    end_f = jnp.broadcast_to(cum_f[:, C - 1:C], (H, C))
    end_b = jnp.broadcast_to(cum_b[:, 0:1], (H, C))
    w_f = jnp.exp(end_f - cum_f + in_f)
    w_b = jnp.exp(end_b - cum_b + in_b)
    rows[0] = cum_f - in_f
    rows[1] = cum_b - in_b
    rows[2] = jnp.exp(in_b)
    turned = jnp.concatenate([cum_f, cum_b, w_f, w_b, jnp.zeros((C - 4 * H, C), F32)], axis=0).T
    wf_hi = w_f.astype(BF16)
    wb_hi = w_b.astype(BF16)
    wf_lo = (w_f - wf_hi.astype(F32)).astype(BF16)
    wb_lo = (w_b - wb_hi.astype(F32)).astype(BF16)
    stacked = jnp.concatenate([wf_hi, wf_lo, wb_hi, wb_lo], axis=0)
    for p in range(PAIRS):
        cols = slice(p * C, (p + 1) * C)
        kp = k_ref[:, cols]
        k32 = kp.astype(F32)
        h0, h1 = 2 * p, 2 * p + 1
        wf = jnp.where(low_half, turned[:, 32 + h0:33 + h0], turned[:, 32 + h1:33 + h1])
        wb = jnp.where(low_half, turned[:, 48 + h0:49 + h0], turned[:, 48 + h1:49 + h1])
        both = jnp.concatenate([k32 * wf, k32 * wb], axis=1).astype(BF16)
        state = lax.dot_general(both, v_ref[:, p * 256:(p + 1) * 256], TN, preferred_element_type=F32).astype(BF16)
        lst[h0, 0] = state[0:64, 0:128]
        lst[h1, 0] = state[64:128, 128:256]
        lst[h0, 1] = state[128:192, 0:128]
        lst[h1, 1] = state[192:256, 128:256]
        norm = jnp.dot(stacked, kp, preferred_element_type=F32)
        norm_f = norm[0:16] + norm[16:32]
        norm_b = norm[32:48] + norm[48:64]
        low_row = low_half[0:1]
        for hh, h in ((0, h0), (1, h1)):
            keep = low_row if hh == 0 else ~low_row
            nf = norm_f[h:h + 1]
            nb = norm_b[h:h + 1]
            nf = jnp.where(keep, nf, pltpu.roll(nf, DK, 1))
            nb = jnp.where(keep, nb, pltpu.roll(nb, DK, 1))
            lsm[h] = jnp.concatenate(
                [nf, nb, end_f[h:h + 1], end_b[h:h + 1], jnp.zeros((4, C), F32)], axis=0)

    each_peer(lambda p: remote(lsm.at[p], rxm.at[me], sc.at[p], rc.at[me], p).start())
    each_peer(lambda p: remote(lst.at[p], rxs.at[me], sb.at[p], rb.at[me], p).start())
    rxs[me] = lst[me]
    rxm[me] = lsm[me]

    for h in range(H):
        fcol[h] = jnp.broadcast_to(turned[:, h:h + 1], (C, C))
        bcol[h] = jnp.broadcast_to(turned[:, 16 + h:17 + h], (C, C))

    def lhs_of(cols):
        qp = q_ref[:, cols] * jnp.asarray(DK ** -0.5, BF16)
        none = jnp.zeros_like(qp)
        return jnp.concatenate([jnp.where(low_half, qp, none), jnp.where(low_half, none, qp)], axis=0)

    def inner_step(p, carry):
        cols = pl.ds(pl.multiple_of(p * C, C), C)
        score2 = lax.dot_general(lhs_of(cols), k_ref[:, cols], NT, preferred_element_type=F32)
        for hh in range(2):
            h = 2 * p + hh
            score = score2[hh * C:(hh + 1) * C]
            ahead = fcol[h] - rows[0, pl.ds(h, 1), :]
            behind = bcol[h] - rows[1, pl.ds(h, 1), :]
            weighted = score * jnp.exp(jnp.where(earlier, ahead, behind))
            pf = jnp.where(earlier, weighted, 0.0)
            pb = jnp.where(earlier, jnp.where(diagonal, score * rows[2, pl.ds(h, 1), :], 0.0), weighted)
            both = jnp.concatenate([pf, pb], axis=0)
            zfb[h] = jnp.broadcast_to(jnp.sum(both, axis=1, keepdims=True), (2 * C, C))
            vcols = pl.ds(pl.multiple_of(h * DV, DV), DV)
            nfb[h] = jnp.dot(both.astype(BF16), v_ref[:, vcols], preferred_element_type=F32)
        return carry

    lax.fori_loop(0, PAIRS, inner_step, 0)

    each_peer(lambda p: remote(lsm.at[p], rxm.at[p], sc.at[p], rc.at[p], p).wait_recv())
    each_peer(lambda p: remote(lst.at[p], rxs.at[p], sb.at[p], rb.at[p], p).wait_recv())

    def carry_step(c, state):
        mf, mb, nf, nb = state
        d = H - 1 - c
        ent[c, 0] = mf.astype(BF16)
        ent[d, 1] = mb.astype(BF16)
        enm[c, 0:1] = nf
        enm[d, 1:2] = nb
        keep_f = jnp.exp(rxm[c, 2:3])
        keep_b = jnp.exp(rxm[d, 3:4])
        return (
            mf * keep_f + rxs[c, 0].astype(F32),
            mb * keep_b + rxs[d, 1].astype(F32),
            nf * keep_f + rxm[c, 0:1],
            nb * keep_b + rxm[d, 1:2],
        )

    zero_m = jnp.zeros((DK, DV), F32)
    zero_n = jnp.zeros((1, C), F32)
    enm[...] = jnp.zeros_like(enm)
    lax.fori_loop(0, H, carry_step, (zero_m, zero_m, zero_n, zero_n))

    def slot(h):
        return est.at[lax.div(h, 2), :, pl.ds(pl.multiple_of(lax.rem(h, 2) * DK, DK), DK), :]

    each_peer(lambda p: remote(enm.at[p], esm.at[me], sd.at[p], rd.at[me], p).start())
    each_peer(lambda p: remote(ent.at[p], slot(me), se.at[p], re.at[me], p).start())
    esm[me] = enm[me]
    est[lax.div(me, 2), :, pl.ds(pl.multiple_of(lax.rem(me, 2) * DK, DK), DK), :] = ent[me]

    def outer_step(p, carry):
        for hh in range(2):
            h = 2 * p + hh

            @pl.when(h != me)
            def _():
                remote(enm.at[h], esm.at[h], sd.at[h], rd.at[h], h).wait_recv()
                remote(ent.at[h], slot(h), se.at[h], re.at[h], h).wait_recv()

        cols = pl.ds(pl.multiple_of(p * C, C), C)
        lhs = lhs_of(cols)
        carried = jnp.dot(lhs, jnp.concatenate([est[p, 0], est[p, 1]], axis=1), preferred_element_type=F32)
        low_row = low_half[0:1]
        nf_row = jnp.where(low_row, esm[2 * p, 0:1], esm[2 * p + 1, 0:1])
        nb_row = jnp.where(low_row, esm[2 * p, 1:2], esm[2 * p + 1, 1:2])
        lhs32 = lhs.astype(F32)
        zf_all = jnp.sum(lhs32 * nf_row, axis=1, keepdims=True)
        zb_all = jnp.sum(lhs32 * nb_row, axis=1, keepdims=True)
        for hh in range(2):
            h = 2 * p + hh
            part = slice(hh * C, (hh + 1) * C)
            grow_f = jnp.exp(fcol[h])
            grow_b = jnp.exp(bcol[h])
            zf = zfb[h, 0:C] + grow_f * zf_all[part]
            zb = zfb[h, C:2 * C] + grow_b * zb_all[part]
            nf = nfb[h, 0:C] + grow_f * carried[part, 0:DV]
            nb = nfb[h, C:2 * C] + grow_b * carried[part, DV:2 * DV]
            total = nf / jnp.maximum(jnp.abs(zf), 1.0) + nb / jnp.maximum(jnp.abs(zb), 1.0)
            mean = jnp.mean(total * total, axis=1, keepdims=True)
            mixed = (total * lax.rsqrt(mean + EPS) * rx1[h, 1:2]).astype(BF16)
            vcols = pl.ds(pl.multiple_of(h * DV, DV), DV)
            out_ref[:, vcols] = (mixed.astype(F32) * sg[:, vcols]).astype(BF16)
        return carry

    lax.fori_loop(0, PAIRS, outer_step, 0)

    each_peer(lambda p: remote(msg_ref.at[p], rx1.at[me], sa.at[p], ra.at[me], p).wait_send())
    each_peer(lambda p: remote(lsm.at[p], rxm.at[me], sc.at[p], rc.at[me], p).wait_send())
    each_peer(lambda p: remote(lst.at[p], rxs.at[me], sb.at[p], rb.at[me], p).wait_send())
    each_peer(lambda p: remote(enm.at[p], esm.at[me], sd.at[p], rd.at[me], p).wait_send())
    each_peer(lambda p: remote(ent.at[p], slot(me), se.at[p], re.at[me], p).wait_send())


def cell(queries, keys, values, gate_logits, retention_offset, log_forget_extra, lane_amplifier, output_gate_logits):
    gates = gate_logits[0].reshape(C, H, 4).transpose(2, 1, 0).astype(F32)
    msg = jnp.concatenate(
        [
            log_forget_extra.reshape(H, 1, C),
            jnp.broadcast_to(lane_amplifier.reshape(1, 1, C), (H, 1, C)),
            jnp.broadcast_to(retention_offset.reshape(1, 2, 1), (H, 2, C)),
            jnp.zeros((H, 4, C), F32),
        ],
        axis=1,
    )
    vm = pl.BlockSpec(memory_space=pltpu.VMEM)
    dma = pltpu.SemaphoreType.DMA((H,))
    return pl.pallas_call(
        cell_kernel,
        out_shape=jax.ShapeDtypeStruct((C, H * DV), BF16),
        in_specs=[vm] * 6,
        out_specs=vm,
        scratch_shapes=[
            pltpu.VMEM((H, 8, C), F32),
            pltpu.VMEM((H, 2, DK, DV), BF16),
            pltpu.VMEM((H, 8, C), F32),
            pltpu.VMEM((H, 2, DK, DV), BF16),
            pltpu.VMEM((H, 8, C), F32),
            pltpu.VMEM((H, 2, DK, DV), BF16),
            pltpu.VMEM((H, 8, C), F32),
            pltpu.VMEM((PAIRS, 2, 2 * DK, DV), BF16),
            pltpu.VMEM((H, 8, C), F32),
            pltpu.VMEM((H, C, C), F32),
            pltpu.VMEM((H, C, C), F32),
            pltpu.VMEM((3, H, C), F32),
            pltpu.VMEM((H, 2 * C, DV), F32),
            pltpu.VMEM((H, 2 * C, C), F32),
            pltpu.VMEM((C, H * DV), F32),
        ] + [dma] * 10,
        compiler_params=pltpu.CompilerParams(
            collective_id=0, has_side_effects=True, vmem_limit_bytes=40 * 1024 * 1024),
        cost_estimate=pl.CostEstimate(flops=20_000_000_000, bytes_accessed=4_000_000, transcendentals=0),
        name="cell",
    )(queries[0], keys[0], values[0], gates, msg, output_gate_logits[0])


def on_device(
    residual_input,
    queries,
    keys,
    values,
    gate_logits,
    retention_offset,
    log_forget_extra,
    lane_amplifier,
    output_gate_logits,
    output_projection,
    cell_norm_gain,
    expert_norm_gain,
    expert_index,
    group_mixing_weight,
    within_group_weight,
    gate_weight,
    up_weight,
    down_weight,
):
    tok_rows = C
    width = residual_input.shape[2]
    gated = cell(queries, keys, values, gate_logits, retention_offset, log_forget_extra, lane_amplifier, output_gate_logits)
    proj = jnp.dot(
        gated,
        lax.all_gather(output_projection, "dp", axis=1, tiled=True),
        preferred_element_type=jnp.float32,
    )
    stream_f = residual_input.reshape(tok_rows, width).astype(jnp.float32)
    stream = (
        stream_f
        + cell_norm_gain * proj * lax.rsqrt(jnp.mean(proj * proj, axis=1, keepdims=True) + EPS)
    ).astype(jnp.bfloat16)
    stream_f = stream.astype(jnp.float32)
    moe_in = (
        expert_norm_gain
        * stream_f
        * lax.rsqrt(jnp.mean(stream_f * stream_f, axis=1, keepdims=True) + EPS)
    ).astype(jnp.bfloat16)
    seq_devices = lax.axis_size("sp")
    seq_groups = lax.axis_size("dp")
    experts = seq_devices * seq_groups
    capacity = 4 * tok_rows // experts
    flat_ids = expert_index.reshape(tok_rows * 2)
    onehot = (flat_ids[:, None] == jnp.arange(experts, dtype=jnp.int32)[None, :]).astype(jnp.int32)
    slot_index = jnp.sum((jnp.cumsum(onehot, axis=0) - onehot) * onehot, axis=1)
    target = flat_ids * capacity + slot_index
    slot_table = (
        target[:, None] == jnp.arange(experts * capacity, dtype=jnp.int32)[None, :]
    ).astype(jnp.bfloat16)
    token_table = jnp.sum(slot_table.reshape(tok_rows, 2, experts * capacity), axis=1)
    outgoing = lax.dot_general(
        token_table, moe_in, (((0,), (0,)), ((), ())), preferred_element_type=jnp.float32
    ).astype(jnp.bfloat16)
    incoming = lax.all_to_all(outgoing, ("sp", "dp"), split_axis=0, concat_axis=0, tiled=True)
    hidden = (
        jax.nn.silu(jnp.dot(incoming, gate_weight[0], preferred_element_type=jnp.float32))
        * jnp.dot(incoming, up_weight[0], preferred_element_type=jnp.float32)
    ).astype(jnp.bfloat16)
    produced = jnp.dot(hidden, down_weight[0], preferred_element_type=jnp.float32).astype(
        jnp.bfloat16
    )
    returned = lax.all_to_all(produced, ("sp", "dp"), split_axis=0, concat_axis=0, tiled=True)
    group_count = group_mixing_weight.shape[2]
    group_of = expert_index.reshape(tok_rows, 2) // (experts // group_count)
    group_hit = (
        group_of[:, :, None] == jnp.arange(group_count, dtype=jnp.int32)[None, None, :]
    ).astype(jnp.float32)
    chosen_group = jnp.sum(
        group_mixing_weight.reshape(tok_rows, 1, group_count) * group_hit, axis=2
    )
    route = chosen_group * within_group_weight.reshape(tok_rows, 2)
    picked = jnp.dot(slot_table, returned, preferred_element_type=jnp.float32).reshape(
        tok_rows, 2, width
    )
    mixture = jnp.sum(picked * route[:, :, None], axis=1)
    return (stream_f + mixture).astype(jnp.bfloat16).reshape(1, tok_rows, width)


def solution(mesh):
    in_specs = (
        P("dp", "sp", None),
        P("dp", "sp", None),
        P("dp", "sp", None),
        P("dp", "sp", None),
        P("dp", "sp", None),
        P("sp", None),
        P("dp", "sp", None),
        P("sp"),
        P("dp", "sp", None),
        P(None, "dp"),
        P(),
        P(),
        P("dp", "sp", None),
        P("dp", "sp", None),
        P("dp", "sp", None),
        P(("sp", "dp"), None, None),
        P(("sp", "dp"), None, None),
        P(("sp", "dp"), None, None),
    )
    out_specs = P("dp", "sp", None)
    return jax.shard_map(
        on_device, mesh=mesh, in_specs=in_specs, out_specs=out_specs, check_vma=False
    )
```

profile of v0, /device:TPU:1, one launch (start us, length us, event | category | flops | bytes accessed | tf_op | source)
XLA Modules:
  0.0 184.0 jit_solution(7963393084228193407)
XLA Ops:
  6.6 0.7 all-gather.2.cloned.1.call-update
  7.3 0.8 copy.31
  8.1 0.1 eq.78
  8.2 0.1 eq.74
  8.4 0.7 pad.2.clone
  9.1 0.1 pad.3.clone
  9.2 0.7 copy.40
  9.9 0.1 copy.34
  10.0 0.2 fusion.28
  10.3 0.2 fusion.30
  10.5 0.1 reduce_sum.61
  10.7 0.1 copy.36
  10.8 0.1 fusion.26
  10.9 0.1 maximum_maximum_fusion.msg_ref
  11.1 31.4 %cell.1 = bf16[128,2048]{1,0:T(8,128)(2,1)S(1)} custom-call(bf16[128,1024]{1,0:T(8,128)(2,1)S(1)} %bitcast.81, bf16[128,1024]{1,0:T(8,128)(2,1)S(1)} %bitcast.82, bf16[128,2048]{1,0:T(8,128)(2,1)S(1)} %bitcast.79, f32[4,16,128]{2,1,0:T(8,128)S(1)} %bitcast.78, f32[16,8,128]{2,1,0:T(8,128)S(1)} %maximum_maximum_fusion.msg_ref, bf16[128,2048]{1,0:T(8,128)(2,1)S(1)} %bitcast.80), custom_call_target="tpu_custom_call" | custom-call | flops 20000000000 | bytes 4000000 | tf_op jit(solution)/shard_map/cell/pallas_call | solution.py:244
  42.5 23.6 %all-gather.2.cloned.1.call-done = bf16[2048,2048]{1,0:T(8,128)(2,1)} async-done(((bf16[2048,256]{1,0:T(8,128)(2,1)}), bf16[2048,2048]{1,0:T(8,128)(2,1)}) %all-gather.2.cloned.1.call-update) | async-done | bytes 8388624 | tf_op jit(solution)/shard_map/all_gather | solution.py:298
  66.1 4.7 %multiply_reduce_fusion = (f32[128]{0:T(128)S(1)}, f32[128,2048]{1,0:T(8,128)S(1)}) fusion(bf16[128,2048]{1,0:T(8,128)(2,1)S(1)} %cell.1, bf16[2048,2048]{1,0:T(8,128)(2,1)} %all-gather.2.cloned.1.call-done), kind=kOutput, calls=%fused_computation.20 | convolution fusion | flops 1074265984 | bytes 9961984 | tf_op jit(solution)/shard_map/dot_general | solution.py:296
  70.8 0.4 fusion.14
  71.2 0.3 copy-done.7
  71.5 0.8 convolution_convert_fusion
  72.3 2.2 %all_to_all.16 = bf16[128,4,2048]{2,1,0:T(4,128)(2,1)} reshape(bf16[512,2048]{1,0:T(8,128)(2,1)S(1)} %convolution_convert_fusion) | data formatting | bytes 4194304 | tf_op jit(solution)/shard_map/all_to_all | solution.py:327
  74.5 39.3 %all_to_all.24 = bf16[128,4,2048]{2,1,0:T(4,128)(2,1)S(1)} all-to-all(bf16[128,4,2048]{2,1,0:T(4,128)(2,1)} %all_to_all.16), channel_id=1, replica_groups=mesh['sp'=16,'dp'=8] {'sp','dp'}, dimensions={0} | all-to-all | bytes 4194304 | tf_op jit(solution)/shard_map/all_to_all | solution.py:327
  113.8 2.0 %all_to_all.18 = bf16[512,2048]{1,0:T(8,128)(2,1)} reshape(bf16[128,4,2048]{2,1,0:T(4,128)(2,1)S(1)} %all_to_all.24) | data formatting | bytes 4194304 | tf_op jit(solution)/shard_map/all_to_all | solution.py:327
  115.9 6.6 %fusion.4 = f32[512,1024]{1,0:T(8,128)} fusion(bf16[512,2048]{1,0:T(8,128)(2,1)} %all_to_all.18, bf16[1,2048,1024]{2,1,0:T(8,128)(2,1)} %param.33), kind=kOutput, calls=%fused_computation.4 | convolution fusion | flops 2147483648 | bytes 8388608 | tf_op jit(solution)/shard_map/dot_general | solution.py:329
  122.5 9.9 %fusion.6 = bf16[512,2048]{1,0:T(8,128)(2,1)} fusion(bf16[1,1024,2048]{2,1,0:T(8,128)(2,1)} %param.35, f32[512,1024]{1,0:T(8,128)} %fusion.4, bf16[512,2048]{1,0:T(8,128)(2,1)S(1)} %copy-done.4, bf16[1,2048,1024]{2,1,0:T(8,128)(2,1)} %param.34), kind=kOutput, calls=%fused_computation.6 | convolution fusion | flops 4299161600 | bytes 14680064 | tf_op jit(solution)/shard_map/dot_general | solution.py:332
  132.4 4.1 %all_to_all.19 = bf16[128,4,2048]{2,1,0:T(4,128)(2,1)} reshape(bf16[512,2048]{1,0:T(8,128)(2,1)} %fusion.6) | data formatting | bytes 4194304 | tf_op jit(solution)/shard_map/all_to_all | solution.py:335
  136.6 4.5 %all-to-all-start.1 = ((bf16[128,4,2048]{2,1,0:T(4,128)(2,1)}), bf16[128,4,2048]{2,1,0:T(4,128)(2,1)S(1)}, u32[]{:S(2)}, u32[]{:S(2)}) async-start(bf16[128,4,2048]{2,1,0:T(4,128)(2,1)} %all_to_all.19), calls=%async_computation.1 | async-start | bytes 4194304 | tf_op jit(solution)/shard_map/all_to_all | solution.py:335
  141.1 0.1 copy.38
  141.2 30.5 %all-to-all-done.1 = bf16[128,4,2048]{2,1,0:T(4,128)(2,1)S(1)} async-done(((bf16[128,4,2048]{2,1,0:T(4,128)(2,1)}), bf16[128,4,2048]{2,1,0:T(4,128)(2,1)S(1)}, u32[]{:S(2)}, u32[]{:S(2)}) %all-to-all-start.1) | async-done | bytes 2097184 | tf_op jit(solution)/shard_map/all_to_all | solution.py:335
  171.7 2.1 %reshape.149 = bf16[512,2048,1]{1,0,2:T(8,128)(2,1)} reshape(bf16[128,4,2048]{2,1,0:T(4,128)(2,1)S(1)} %all-to-all-done.1) | data formatting | bytes 4194304 | tf_op jit(solution)/shard_map/all_to_all | solution.py:335
  173.8 2.5 %fusion.11 = f32[128,2048]{1,0:T(8,128)S(1)} fusion(bf16[512,2048,1]{1,0,2:T(8,128)(2,1)} %reshape.149, f32[128,2]{0,1:T(2,128)S(1)} %bitcast_multiply_fusion.1, s32[128,2]{0,1:T(2,128)S(1)} %copy.36), kind=kOutput, calls=%fused_computation.13 | convolution fusion | flops 537788416 | bytes 3147776 | tf_op jit(solution)/shard_map/dot_general | solution.py:345
  176.3 0.9 fusion.19
  (37 shorter events, 0.3 us)
Async XLA Ops:
  6.5 4.4 %copy-start.8 = (f32[1,1,2048]{2,1,0:T(1,128)S(1)}, f32[1,1,2048]{2,1,0:T(1,128)}, u32[]{:S(2)}) copy-start(f32[1,1,2048]{2,1,0:T(1,128)} %param.24) | copy-start | bytes 24580
  6.5 4.4 %copy-start.11 = (f32[128]{0:T(128)S(1)}, f32[128]{0:T(128)}, u32[]{:S(2)}) copy-start(f32[128]{0:T(128)} %param.25) | copy-start | bytes 1540
  6.5 4.5 %copy-start.1 = (bf16[1,128,2048]{2,1,0:T(8,128)(2,1)S(1)}, bf16[1,128,2048]{2,1,0:T(8,128)(2,1)}, u32[]{:S(2)}) copy-start(bf16[1,128,2048]{2,1,0:T(8,128)(2,1)} %param.26) | copy-start | bytes 1572868
  6.5 4.5 %copy-start = (bf16[1,128,2048]{2,1,0:T(8,128)(2,1)S(1)}, bf16[1,128,2048]{2,1,0:T(8,128)(2,1)}, u32[]{:S(2)}) copy-start(bf16[1,128,2048]{2,1,0:T(8,128)(2,1)} %param.21) | copy-start | bytes 1572868
  6.5 4.5 %copy-start.3 = (bf16[1,128,1024]{2,1,0:T(8,128)(2,1)S(1)}, bf16[1,128,1024]{2,1,0:T(8,128)(2,1)}, u32[]{:S(2)}) copy-start(bf16[1,128,1024]{2,1,0:T(8,128)(2,1)} %param.20) | copy-start | bytes 786436
  6.5 4.5 %copy-start.2 = (bf16[1,128,1024]{2,1,0:T(8,128)(2,1)S(1)}, bf16[1,128,1024]{2,1,0:T(8,128)(2,1)}, u32[]{:S(2)}) copy-start(bf16[1,128,1024]{2,1,0:T(8,128)(2,1)} %param.19) | copy-start | bytes 786436
  6.6 59.5 %all-gather.2.cloned.1.call-start = ((), (), s32[]{:S(2)}) async-start(), calls=%async_computation.2 | async-start | bytes 9437184 | tf_op jit(solution)/shard_map/all_gather | solution.py:298
  42.5 28.3 %copy-start.5 = (bf16[1,128,2048]{2,1,0:T(8,128)(2,1)S(1)}, bf16[1,128,2048]{2,1,0:T(8,128)(2,1)}, u32[]{:S(2)}) copy-start(bf16[1,128,2048]{2,1,0:T(8,128)(2,1)} %param.18) | copy-start | bytes 1572868
  42.5 28.3 %copy-start.6 = (f32[2048]{0:T(1024)S(1)}, f32[2048]{0:T(1024)}, u32[]{:S(2)}) copy-start(f32[2048]{0:T(1024)} %param.28) | copy-start | bytes 24580
  70.8 0.7 copy-start.7
  115.9 6.7 %copy-start.4 = (bf16[512,2048]{1,0:T(8,128)(2,1)S(1)}, bf16[512,2048]{1,0:T(8,128)(2,1)}, u32[]{:S(2)}) copy-start(bf16[512,2048]{1,0:T(8,128)(2,1)} %all_to_all.18) | copy-start | bytes 6291460
  136.6 4.6 %copy-start.9 = (f32[1,128,4]{1,2,0:T(4,128)S(1)}, f32[1,128,4]{1,2,0:T(4,128)}, u32[]{:S(2)}) copy-start(f32[1,128,4]{1,2,0:T(4,128)} %param.31) | copy-start | bytes 6148
  136.6 4.6 %copy-start.10 = (f32[1,128,2]{1,2,0:T(2,128)S(1)}, f32[1,128,2]{1,2,0:T(2,128)}, u32[]{:S(2)}) copy-start(f32[1,128,2]{1,2,0:T(2,128)} %param.32) | copy-start | bytes 3076
  136.6 35.1 %all-to-all-start.1 = ((bf16[128,4,2048]{2,1,0:T(4,128)(2,1)}), bf16[128,4,2048]{2,1,0:T(4,128)(2,1)S(1)}, u32[]{:S(2)}, u32[]{:S(2)}) async-start(bf16[128,4,2048]{2,1,0:T(4,128)(2,1)} %all_to_all.19), calls=%async_computation.1 | async-start | bytes 4194304 | tf_op jit(solution)/shard_map/all_to_all | solution.py:335
Sparse Core Ops, SparseCore 0:
  9.0 56.9 all-gather.1
where the time goes:
time: 185 us; the launch traced here: 184 us
  waiting for transfers between devices  54.7 us (30%)
  blocking collectives  39.3 us (21%)
  Pallas kernels  31.4 us (17%)
  matrix products  24.6 us (13%)
  local copies, waits for them, and re-layouts  13.8 us (7%)
  between operations  13.6 us (7%)
  starting transfers between devices  4.57 us (2%)
  other arithmetic  2.03 us (1%)
    all_to_all x1, blocking collectives, on_device(): lax.all_to_all(outgoing, ('sp', 'dp'), split_axis=0, concat_axis=0, tiled...  39.3 us
    pallas_call x1, Pallas kernels, cell(): pl.pallas_call(cell_kernel, out_shape=jax.ShapeDtypeStruct((C, H * DV), B...  31.4 us
    all_to_all x1, waiting for transfers between devices, on_device(): lax.all_to_all(produced, ('sp', 'dp'), split_axis=0, concat_axis=0, tiled...  30.5 us
    all_gather x1, waiting for transfers between devices, on_device(): lax.all_gather(output_projection, 'dp', axis=1, tiled=True)  23.6 us
    dot_general x1, matrix products, on_device(): jnp.dot(hidden, down_weight[0], preferred_element_type=jnp.float32)  9.9 us
    dot_general x1, matrix products, on_device(): jnp.dot(incoming, gate_weight[0], preferred_element_type=jnp.float32)  6.65 us
    all_to_all x2, local copies, waits for them, and re-layouts, on_device(): lax.all_to_all(produced, ('sp', 'dp'), split_axis=0, concat_axis=0, tiled...  6.17 us
    dot_general x1, matrix products, on_device(): jnp.dot(gated, lax.all_gather(output_projection, 'dp', axis=1, tiled=True...  4.72 us
  transfers between devices with their start and end apart: 2, of which 2 were waited for; matrix products, arithmetic and copies ran while one was open for 2% of the time, Pallas kernels for 17%

commit v1 on v0

v1 whole, which is shorter than its diff:
```python
import jax
import jax.numpy as jnp
from jax import lax
from jax.experimental import pallas as pl
from jax.experimental.pallas import tpu as pltpu
from jax.sharding import PartitionSpec as P

EPS = 1e-06
HIGH = lax.Precision.HIGHEST
F32 = jnp.float32
BF16 = jnp.bfloat16
H = 16
DK = 64
DV = 128
C = 128
D = 2048
FF = 1024
CAP = 4
DEVICES = 128
CHUNKS = 4
PER = DEVICES // CHUNKS
PAIRS = H // 2
STRIDE = 11
QUARTER = D // 4
NT = (((1,), (1,)), ((), ()))
TN = (((0,), (0,)), ((), ()))
MESH = pl.DeviceIdType.MESH


def log_sigmoid(x):
    return jnp.minimum(x, 0.0) - jnp.log1p(jnp.exp(-jnp.abs(x)))


def layer_kernel(
    q_hbm, k_hbm, v_hbm, ogl_hbm, res_hbm, wo_hbm, gate_hbm, up_hbm, down_hbm,
    g_ref, ext_ref, lam_ref, ro_ref, ids_ref, group_ref, within_ref, cng_ref, eng_ref,
    out_ref,
    q_ref, k_ref, v_ref, ogl_ref, res_ref, wbuf, gate_w, up_w, down_w,
    msg, rx1, lst, lsm, rxs, rxm, ent, enm, est, esm,
    gates, fcol, bcol, rows, nfb, zfb, sg,
    gated, proj, tab_send, tab_back, outgoing, arrived, produced, returned,
    loc, sa, ra, sb, rb, sc, rc, sd, rd, se, re,
    wsr, wsl, wrl, wrr, wps, wpr, ds, dr, bs, br,
):
    me = lax.axis_index("sp")
    dp = lax.axis_index("dp")
    z, y = lax.div(me, 4), lax.rem(me, 4)
    x, core = lax.div(dp, 2), lax.rem(dp, 2)
    flat = me * 8 + dp

    def peer_of(d):
        return lax.rem(me + d, H)

    def copy_to(src, dst, ssem, rsem, where):
        return pltpu.make_async_remote_copy(
            src_ref=src, dst_ref=dst, send_sem=ssem, recv_sem=rsem,
            device_id=where, device_id_type=MESH,
        )

    def remote(src, dst, ssem, rsem, peer):
        return copy_to(src, dst, ssem, rsem, (peer, dp))

    def each_peer(body):
        def step(d, carry):
            body(peer_of(d))
            return carry

        lax.fori_loop(1, H, step, 0)

    local = [
        pltpu.make_async_copy(src, dst, loc.at[i])
        for i, (src, dst) in enumerate((
            (wo_hbm, wbuf.at[dp]), (k_hbm, k_ref), (v_hbm, v_ref), (ogl_hbm, ogl_ref), (q_hbm, q_ref),
            (res_hbm, res_ref), (gate_hbm, gate_w), (up_hbm, up_w), (down_hbm, down_w),
        ))
    ]
    for c in local[:5]:
        c.start()

    barrier = pltpu.get_barrier_semaphore()

    def greet(d, carry):
        other = lax.rem(flat + d, DEVICES)
        pl.semaphore_signal(barrier, inc=1, device_id=(lax.div(other, 8), lax.rem(other, 8)), device_id_type=MESH)
        return carry

    lax.fori_loop(1, DEVICES, greet, 0)

    lane = lax.broadcasted_iota(jnp.int32, (C, C), 1)
    row_id = lax.broadcasted_iota(jnp.int32, (C, C), 0)
    low_half = lane < DK
    low_row = low_half[0:1]
    earlier = lane <= row_id
    diagonal = lane == row_id

    msg[:, 0, :] = ext_ref[...]
    msg[:, 1, :] = jnp.broadcast_to(lam_ref[...], (H, C))
    msg[:, 2, :] = jnp.broadcast_to(ro_ref[:, 0:1], (H, C))
    msg[:, 3, :] = jnp.broadcast_to(ro_ref[:, 1:2], (H, C))
    for i in range(4, 8):
        msg[:, i, :] = jnp.zeros((H, C), F32)
    gates[...] = g_ref[...].astype(F32)
    for c in local[:5]:
        c.wait()
    pl.semaphore_wait(barrier, DEVICES - 1)

    each_peer(lambda p: remote(msg.at[p], rx1.at[me], sa.at[p], ra.at[me], p).start())
    rx1[me] = msg[me]

    right = lax.rem(x + 1, 4) * 2 + core
    left = lax.rem(x + 3, 4) * 2 + core
    across = lax.rem(x + 2, 4) * 2 + core
    partner = x * 2 + 1 - core

    def piece(shard, i):
        return wbuf.at[shard, pl.ds(i * QUARTER, QUARTER), :]

    def to_right(shard, i, n):
        return copy_to(piece(shard, i), piece(shard, i), wsr.at[n], wrl.at[n], (me, right))

    def to_left(shard, i, n):
        return copy_to(piece(shard, i), piece(shard, i), wsl.at[n], wrr.at[n], (me, left))

    def to_partner(ref, n):
        return copy_to(ref, ref, wps.at[n], wpr.at[n], (me, partner))

    for n in range(4):
        to_right(dp, n, n).start()
        to_left(dp, (n + 2) % 4, n).start()
    to_partner(wbuf.at[dp], 0).start()
    for c in local[5:]:
        c.start()

    def gate_step(p, carry):
        cols = pl.ds(pl.multiple_of(p * 256, 256), 256)
        sg[:, cols] = 1.0 / (1.0 + jnp.exp(-ogl_ref[:, cols].astype(F32)))
        return carry

    lax.fori_loop(0, PAIRS, gate_step, 0)

    each_peer(lambda p: remote(msg.at[p], rx1.at[p], sa.at[p], ra.at[p], p).wait_recv())

    spread = rx1[:, 0, :]
    in_f = gates[pl.ds(0, H, stride=4), :]
    in_b = gates[pl.ds(2, H, stride=4), :]
    fade_f = log_sigmoid(gates[pl.ds(1, H, stride=4), :] + rx1[:, 2, :]) + spread
    fade_b = log_sigmoid(gates[pl.ds(3, H, stride=4), :] + rx1[:, 3, :]) + spread
    upto = (row_id <= lane).astype(F32)
    since = (row_id >= lane).astype(F32)
    cum_f = jnp.dot(fade_f, upto, precision=HIGH, preferred_element_type=F32)
    cum_b = jnp.dot(fade_b, since, precision=HIGH, preferred_element_type=F32)
    end_f = jnp.broadcast_to(cum_f[:, C - 1:C], (H, C))
    end_b = jnp.broadcast_to(cum_b[:, 0:1], (H, C))
    w_f = jnp.exp(end_f - cum_f + in_f)
    w_b = jnp.exp(end_b - cum_b + in_b)
    rows[0] = cum_f - in_f
    rows[1] = cum_b - in_b
    rows[2] = jnp.exp(in_b)
    turned = jnp.concatenate([cum_f, cum_b, w_f, w_b, jnp.zeros((C - 4 * H, C), F32)], axis=0).T
    wf_hi = w_f.astype(BF16)
    wb_hi = w_b.astype(BF16)
    wf_lo = (w_f - wf_hi.astype(F32)).astype(BF16)
    wb_lo = (w_b - wb_hi.astype(F32)).astype(BF16)
    stacked = jnp.concatenate([wf_hi, wf_lo, wb_hi, wb_lo], axis=0)
    for p in range(PAIRS):
        kp = k_ref[:, p * C:(p + 1) * C]
        k32 = kp.astype(F32)
        h0, h1 = 2 * p, 2 * p + 1
        wf = jnp.where(low_half, turned[:, 32 + h0:33 + h0], turned[:, 32 + h1:33 + h1])
        wb = jnp.where(low_half, turned[:, 48 + h0:49 + h0], turned[:, 48 + h1:49 + h1])
        both = jnp.concatenate([k32 * wf, k32 * wb], axis=1).astype(BF16)
        state = lax.dot_general(both, v_ref[:, p * 256:(p + 1) * 256], TN, preferred_element_type=F32).astype(BF16)
        lst[h0, 0] = state[0:64, 0:128]
        lst[h1, 0] = state[64:128, 128:256]
        lst[h0, 1] = state[128:192, 0:128]
        lst[h1, 1] = state[192:256, 128:256]
        norm = jnp.dot(stacked, kp, preferred_element_type=F32)
        norm_f = norm[0:16] + norm[16:32]
        norm_b = norm[32:48] + norm[48:64]
        for h, keep in ((h0, low_row), (h1, ~low_row)):
            nf = norm_f[h:h + 1]
            nb = norm_b[h:h + 1]
            nf = jnp.where(keep, nf, pltpu.roll(nf, DK, 1))
            nb = jnp.where(keep, nb, pltpu.roll(nb, DK, 1))
            lsm[h] = jnp.concatenate(
                [nf, nb, end_f[h:h + 1], end_b[h:h + 1], jnp.zeros((4, C), F32)], axis=0)

    each_peer(lambda p: remote(lsm.at[p], rxm.at[me], sc.at[p], rc.at[me], p).start())
    each_peer(lambda p: remote(lst.at[p], rxs.at[me], sb.at[p], rb.at[me], p).start())
    rxs[me] = lst[me]
    rxm[me] = lsm[me]

    for h in range(H):
        fcol[h] = jnp.broadcast_to(turned[:, h:h + 1], (C, C))
        bcol[h] = jnp.broadcast_to(turned[:, 16 + h:17 + h], (C, C))

    def lhs_of(cols):
        qp = q_ref[:, cols] * jnp.asarray(DK ** -0.5, BF16)
        none = jnp.zeros_like(qp)
        return jnp.concatenate([jnp.where(low_half, qp, none), jnp.where(low_half, none, qp)], axis=0)

    def inner_step(p, carry):
        cols = pl.ds(pl.multiple_of(p * C, C), C)
        score2 = lax.dot_general(lhs_of(cols), k_ref[:, cols], NT, preferred_element_type=F32)
        for hh in range(2):
            h = 2 * p + hh
            score = score2[hh * C:(hh + 1) * C]
            ahead = fcol[h] - rows[0, pl.ds(h, 1), :]
            behind = bcol[h] - rows[1, pl.ds(h, 1), :]
            weighted = score * jnp.exp(jnp.where(earlier, ahead, behind))
            pf = jnp.where(earlier, weighted, 0.0)
            pb = jnp.where(earlier, jnp.where(diagonal, score * rows[2, pl.ds(h, 1), :], 0.0), weighted)
            both = jnp.concatenate([pf, pb], axis=0)
            zfb[h] = jnp.broadcast_to(jnp.sum(both, axis=1, keepdims=True), (2 * C, C))
            vcols = pl.ds(pl.multiple_of(h * DV, DV), DV)
            nfb[h] = jnp.dot(both.astype(BF16), v_ref[:, vcols], preferred_element_type=F32)
        return carry

    lax.fori_loop(0, PAIRS, inner_step, 0)

    each_peer(lambda p: remote(lsm.at[p], rxm.at[p], sc.at[p], rc.at[p], p).wait_recv())
    each_peer(lambda p: remote(lst.at[p], rxs.at[p], sb.at[p], rb.at[p], p).wait_recv())

    enm[...] = jnp.zeros_like(enm)

    def carry_step(c, state):
        mf, mb, nf, nb = state
        d = H - 1 - c
        ent[c, 0] = mf.astype(BF16)
        ent[d, 1] = mb.astype(BF16)
        enm[c, 0:1] = nf
        enm[d, 1:2] = nb
        keep_f = jnp.exp(rxm[c, 2:3])
        keep_b = jnp.exp(rxm[d, 3:4])
        return (
            mf * keep_f + rxs[c, 0].astype(F32),
            mb * keep_b + rxs[d, 1].astype(F32),
            nf * keep_f + rxm[c, 0:1],
            nb * keep_b + rxm[d, 1:2],
        )

    zero_m = jnp.zeros((DK, DV), F32)
    zero_n = jnp.zeros((1, C), F32)
    lax.fori_loop(0, H, carry_step, (zero_m, zero_m, zero_n, zero_n))

    def slot(h):
        return est.at[lax.div(h, 2), :, pl.ds(pl.multiple_of(lax.rem(h, 2) * DK, DK), DK), :]

    each_peer(lambda p: remote(enm.at[p], esm.at[me], sd.at[p], rd.at[me], p).start())
    each_peer(lambda p: remote(ent.at[p], slot(me), se.at[p], re.at[me], p).start())
    esm[me] = enm[me]
    est[lax.div(me, 2), :, pl.ds(pl.multiple_of(lax.rem(me, 2) * DK, DK), DK), :] = ent[me]

    for n in range(2):
        to_right(left, n, n).wait_recv()
        to_right(left, n, 4 + n).start()
        to_left(right, n + 2, n).wait_recv()
        to_left(right, n + 2, 4 + n).start()

    table_in = jnp.concatenate(
        [ids_ref[...].astype(F32), group_ref[...], within_ref[...], jnp.zeros((C - 8, C), F32)], axis=0).T
    wide = lax.broadcasted_iota(jnp.int32, (C, DEVICES * CAP), 1)
    hits, targets, routes = [], [], []
    for n in range(2):
        expert = table_in[:, n:n + 1].astype(jnp.int32)
        dz = jnp.bitwise_and(jnp.right_shift(expert, 5) - z + 4, 3)
        dy = jnp.bitwise_and(jnp.right_shift(expert, 3) - y + 8, 3)
        dx = jnp.bitwise_and(jnp.right_shift(expert, 1) - x + 4, 3)
        dc = jnp.bitwise_and(expert - core + 2, 1)
        place = jnp.bitwise_and(dz + dy + dx, 3) * PER + dy * 8 + dx * 2 + dc
        group = jnp.right_shift(expert, 5)
        share = jnp.zeros((C, 1), F32)
        for i in range(4):
            share = share + jnp.where(group == i, table_in[:, 2 + i:3 + i], 0.0)
        routes.append(share * table_in[:, 6 + n:7 + n])
        targets.append(place * CAP)
        hits.append((lane == place).astype(F32))
    before = jnp.dot((lane < row_id).astype(BF16), (hits[0] + hits[1]).astype(BF16), preferred_element_type=F32)
    sent = jnp.zeros((C, DEVICES * CAP), F32)
    back = jnp.zeros((C, DEVICES * CAP), F32)
    for n in range(2):
        nth = jnp.sum(before * hits[n], axis=1, keepdims=True).astype(jnp.int32)
        chosen = wide == targets[n] + nth
        sent = sent + jnp.where(chosen, 1.0, 0.0)
        back = back + jnp.where(chosen, routes[n], 0.0)
    tab_send[...] = sent.astype(BF16)
    back_hi = back.astype(BF16)
    tab_back[0:C] = back_hi
    tab_back[C:2 * C] = (back - back_hi.astype(F32)).astype(BF16)

    def outer_step(p, carry):
        for hh in range(2):
            h = 2 * p + hh

            @pl.when(h != me)
            def _():
                remote(enm.at[h], esm.at[h], sd.at[h], rd.at[h], h).wait_recv()
                remote(ent.at[h], slot(h), se.at[h], re.at[h], h).wait_recv()

        cols = pl.ds(pl.multiple_of(p * C, C), C)
        lhs = lhs_of(cols)
        carried = jnp.dot(lhs, jnp.concatenate([est[p, 0], est[p, 1]], axis=1), preferred_element_type=F32)
        nf_row = jnp.where(low_row, esm[2 * p, 0:1], esm[2 * p + 1, 0:1])
        nb_row = jnp.where(low_row, esm[2 * p, 1:2], esm[2 * p + 1, 1:2])
        lhs32 = lhs.astype(F32)
        zf_all = jnp.sum(lhs32 * nf_row, axis=1, keepdims=True)
        zb_all = jnp.sum(lhs32 * nb_row, axis=1, keepdims=True)
        for hh in range(2):
            h = 2 * p + hh
            part = slice(hh * C, (hh + 1) * C)
            grow_f = jnp.exp(fcol[h])
            grow_b = jnp.exp(bcol[h])
            zf = zfb[h, 0:C] + grow_f * zf_all[part]
            zb = zfb[h, C:2 * C] + grow_b * zb_all[part]
            nf = nfb[h, 0:C] + grow_f * carried[part, 0:DV]
            nb = nfb[h, C:2 * C] + grow_b * carried[part, DV:2 * DV]
            total = nf / jnp.maximum(jnp.abs(zf), 1.0) + nb / jnp.maximum(jnp.abs(zb), 1.0)
            mean = jnp.mean(total * total, axis=1, keepdims=True)
            mixed = (total * lax.rsqrt(mean + EPS) * rx1[h, 1:2]).astype(BF16)
            vcols = pl.ds(pl.multiple_of(h * DV, DV), DV)
            gated[:, vcols] = (mixed.astype(F32) * sg[:, vcols]).astype(BF16)
        return carry

    lax.fori_loop(0, PAIRS, outer_step, 0)

    def project(shard):
        cols = pl.ds(pl.multiple_of(shard * 256, 256), 256)
        proj[:, cols] = jnp.dot(gated[...], wbuf[shard], preferred_element_type=F32)

    project(dp)
    for n in range(2, 4):
        to_right(left, n, n).wait_recv()
        to_left(right, n - 2, n).wait_recv()
    to_partner(wbuf.at[left], 1).start()
    to_partner(wbuf.at[right], 2).start()
    project(left)
    project(right)
    far = 1 - 2 * core
    to_partner(wbuf.at[partner], 0).wait_recv()
    project(partner)
    for n in range(2):
        to_right(across, n, 4 + n).wait_recv()
        to_partner(piece(across, n), 3 + n).start()
        to_left(across, n + 2, 4 + n).wait_recv()
        to_partner(piece(across, n + 2), 5 + n).start()
    to_partner(wbuf.at[left + far], 1).wait_recv()
    project(left + far)
    to_partner(wbuf.at[right + far], 2).wait_recv()
    project(right + far)
    project(across)
    for n in range(2):
        to_partner(piece(across + far, n), 3 + n).wait_recv()
        to_partner(piece(across + far, n + 2), 5 + n).wait_recv()
    project(across + far)

    local[5].wait()
    pr = proj[...]
    scale = lax.rsqrt(jnp.mean(pr * pr, axis=1, keepdims=True) + EPS)
    stream = (res_ref[...].astype(F32) + cng_ref[...] * pr * scale).astype(BF16).astype(F32)
    proj[...] = stream
    scale = lax.rsqrt(jnp.mean(stream * stream, axis=1, keepdims=True) + EPS)
    gated[...] = (eng_ref[...] * stream * scale).astype(BF16)

    def route_of(j, i):
        t = lax.rem(i * STRIDE, PER)
        dc = lax.rem(t, 2)
        dx = lax.rem(lax.div(t, 2), 4)
        dy = lax.div(t, 8)
        dz = lax.rem(j + 8 - dx - dy, 4)
        return j * PER + t, dz, dy, dx, dc

    def onward(j, i):
        place, dz, dy, dx, dc = route_of(j, i)
        sp_to = lax.rem(z + dz, 4) * 4 + lax.rem(y + dy, 4)
        dp_to = lax.rem(x + dx, 4) * 2 + lax.rem(core + dc, 2)
        return place, (sp_to, dp_to)

    def homeward(j, i):
        place, dz, dy, dx, dc = route_of(j, i)
        sp_to = lax.rem(z + 4 - dz, 4) * 4 + lax.rem(y + 4 - dy, 4)
        dp_to = lax.rem(x + 4 - dx, 4) * 2 + lax.rem(core + dc, 2)
        return place, (sp_to, dp_to)

    def send_chunk(j, way, src, dst, ssem, rsem):
        def step(i, carry):
            place, where = way(j, i)

            @pl.when(place != 0)
            def _():
                copy_to(src.at[place], dst.at[place], ssem.at[j], rsem.at[j], where).start()

            return carry

        lax.fori_loop(0, PER, step, 0)

    def whole(j, src, dst, ssem, rsem):
        span = pl.ds(1, PER - 1) if j == 0 else pl.ds(j * PER, PER)
        return copy_to(src.at[span], dst.at[span], ssem.at[j], rsem.at[j], (me, partner))

    for j in range(CHUNKS):
        rows_out = lax.dot_general(
            tab_send[:, j * C:(j + 1) * C], gated[...], TN, preferred_element_type=F32)
        outgoing[j * PER:(j + 1) * PER] = rows_out.astype(BF16).reshape(PER, CAP, D)
        send_chunk(j, onward, outgoing, arrived, ds, dr)
        if j == 0:
            arrived[0] = outgoing[0]

    for c in local[6:]:
        c.wait()

    def expert_chunk(j):
        rows_in = arrived[pl.ds(j * PER, PER)].reshape(PER * CAP, D)
        a = jnp.dot(rows_in, gate_w[...], preferred_element_type=F32)
        b = jnp.dot(rows_in, up_w[...], preferred_element_type=F32)
        hidden = (a / (1.0 + jnp.exp(-a)) * b).astype(BF16)
        made = jnp.dot(hidden, down_w[...], preferred_element_type=F32).astype(BF16)
        produced[pl.ds(j * PER, PER)] = made.reshape(PER, CAP, D)

    def expert_step(j, carry):
        for n in range(CHUNKS):
            @pl.when(j == n)
            def _():
                whole(n, outgoing, arrived, ds, dr).wait_recv()

        expert_chunk(j)
        send_chunk(j, homeward, produced, returned, bs, br)
        return carry

    lax.fori_loop(0, CHUNKS, expert_step, 0)
    returned[0] = produced[0]

    for j in range(CHUNKS):
        whole(j, produced, returned, bs, br).wait_recv()
        rows_back = returned[j * PER:(j + 1) * PER].reshape(PER * CAP, D)
        parts = jnp.dot(tab_back[:, j * C:(j + 1) * C], rows_back, preferred_element_type=F32)
        proj[...] += parts[0:C] + parts[C:2 * C]
    out_ref[...] = proj[...].astype(BF16)

    each_peer(lambda p: remote(msg.at[p], rx1.at[me], sa.at[p], ra.at[me], p).wait_send())
    each_peer(lambda p: remote(lsm.at[p], rxm.at[me], sc.at[p], rc.at[me], p).wait_send())
    each_peer(lambda p: remote(lst.at[p], rxs.at[me], sb.at[p], rb.at[me], p).wait_send())
    each_peer(lambda p: remote(enm.at[p], esm.at[me], sd.at[p], rd.at[me], p).wait_send())
    each_peer(lambda p: remote(ent.at[p], slot(me), se.at[p], re.at[me], p).wait_send())
    for n in range(6):
        to_right(dp, 0, n).wait_send()
        to_left(dp, 0, n).wait_send()
    for n in range(3):
        to_partner(wbuf.at[dp], n).wait_send()
    for n in range(3, 7):
        to_partner(piece(dp, 0), n).wait_send()
    for j in range(CHUNKS):
        whole(j, outgoing, arrived, ds, dr).wait_send()
        whole(j, produced, returned, bs, br).wait_send()


def on_device(
    residual_input, queries, keys, values, gate_logits, retention_offset, log_forget_extra,
    lane_amplifier, output_gate_logits, output_projection, cell_norm_gain, expert_norm_gain,
    expert_index, group_mixing_weight, within_group_weight, gate_weight, up_weight, down_weight,
):
    vm = pl.BlockSpec(memory_space=pltpu.VMEM)
    hbm = pl.BlockSpec(memory_space=pl.ANY)
    dma = pltpu.SemaphoreType.DMA
    small = pltpu.VMEM((H, 8, C), F32)
    state = pltpu.VMEM((H, 2, DK, DV), BF16)
    slots = pltpu.VMEM((DEVICES, CAP, D), BF16)
    out = pl.pallas_call(
        layer_kernel,
        out_shape=jax.ShapeDtypeStruct((C, D), BF16),
        in_specs=[hbm] * 9 + [vm] * 9,
        out_specs=vm,
        scratch_shapes=[
            pltpu.VMEM((C, H * DK), BF16),
            pltpu.VMEM((C, H * DK), BF16),
            pltpu.VMEM((C, H * DV), BF16),
            pltpu.VMEM((C, H * DV), BF16),
            pltpu.VMEM((C, D), BF16),
            pltpu.VMEM((8, D, 256), BF16),
            pltpu.VMEM((D, FF), BF16),
            pltpu.VMEM((D, FF), BF16),
            pltpu.VMEM((FF, D), BF16),
            small, small, state, small, state, small, state, small,
            pltpu.VMEM((PAIRS, 2, 2 * DK, DV), BF16),
            small,
            pltpu.VMEM((4 * H, C), F32),
            pltpu.VMEM((H, C, C), F32),
            pltpu.VMEM((H, C, C), F32),
            pltpu.VMEM((3, H, C), F32),
            pltpu.VMEM((H, 2 * C, DV), F32),
            pltpu.VMEM((H, 2 * C, C), F32),
            pltpu.VMEM((C, H * DV), F32),
            pltpu.VMEM((C, H * DV), BF16),
            pltpu.VMEM((C, D), F32),
            pltpu.VMEM((C, DEVICES * CAP), BF16),
            pltpu.VMEM((2 * C, DEVICES * CAP), BF16),
            slots, slots, slots, slots,
            dma((9,)),
        ] + [dma((H,))] * 10 + [dma((6,))] * 4 + [dma((7,))] * 2 + [dma((CHUNKS,))] * 4,
        compiler_params=pltpu.CompilerParams(
            collective_id=0, has_side_effects=True, vmem_limit_bytes=67_043_328),
        name="layer",
    )(
        queries[0], keys[0], values[0], output_gate_logits[0], residual_input[0], output_projection,
        gate_weight[0], up_weight[0], down_weight[0],
        gate_logits[0].T, log_forget_extra.reshape(H, C), lane_amplifier.reshape(1, C), retention_offset,
        expert_index[0].T, group_mixing_weight[0].T, within_group_weight[0].T,
        cell_norm_gain.reshape(1, D), expert_norm_gain.reshape(1, D),
    )
    return out.reshape(1, C, D)


def solution(mesh):
    by_place = P("dp", "sp", None)
    by_expert = P(("sp", "dp"), None, None)
    in_specs = (
        by_place, by_place, by_place, by_place, by_place, P("sp", None), by_place, P("sp"), by_place,
        P(None, "dp"), P(), P(), by_place, by_place, by_place, by_expert, by_expert, by_expert,
    )
    return jax.shard_map(on_device, mesh=mesh, in_specs=in_specs, out_specs=by_place, check_vma=False)
```

time: 185 us -> 105 us (0.57)
  Pallas kernels: 31.4 us -> 103 us
  waiting for transfers between devices: 54.7 us -> 0 us
  blocking collectives: 39.3 us -> 0 us
  matrix products: 24.6 us -> 0 us
  between operations: 13.6 us -> 0.01 us
  local copies, waits for them, and re-layouts: 13.8 us -> 1.88 us
  starting transfers between devices: 4.57 us -> 0 us
  other arithmetic: 2.03 us -> 0 us
    pallas_call x1, Pallas kernels: 31.4 us -> 103 us  [on_device(): pl.pallas_call(layer_kernel, out_shape=jax.ShapeDtypeStruct((C, D), BF16)...]
    all_to_all x1 -> x0, blocking collectives: 39.3 us -> none  [on_device(): lax.all_to_all(outgoing, ('sp', 'dp'), split_axis=0, concat_axis=0, tiled...]
    all_to_all x1 -> x0, waiting for transfers between devices: 30.5 us -> none  [on_device(): lax.all_to_all(produced, ('sp', 'dp'), split_axis=0, concat_axis=0, tiled...]
    dot_general x5 -> x0, matrix products: 24.6 us -> none  [the longest x1 9.9 us: on_device(): jnp.dot(hidden, down_weight[0], preferred_element_type=jnp.float32)]
    all_gather x1 -> x0, waiting for transfers between devices: 23.6 us -> none  [on_device(): lax.all_gather(output_projection, 'dp', axis=1, tiled=True)]
    all_to_all x4 -> x0, local copies, waits for them, and re-layouts: 10.4 us -> none  [the longest x2 6.17 us: on_device(): lax.all_to_all(produced, ('sp', 'dp'), split_axis=0, concat_axis=0, tiled...]
    all_to_all x1 -> x0, starting transfers between devices: 4.53 us -> none  [on_device(): lax.all_to_all(produced, ('sp', 'dp'), split_axis=0, concat_axis=0, tiled...]
  transfers between devices with their start and end apart: 2 -> 0, of which waited for: 2 -> 0; matrix products, arithmetic and copies ran while one was open for 2% -> 0% of each run, Pallas kernels for 17% -> 0%
where the time goes in v1:
time: 105 us
  Pallas kernels  103 us (98%)
  local copies, waits for them, and re-layouts  1.88 us (2%)
    pallas_call x1, Pallas kernels, on_device(): pl.pallas_call(layer_kernel, out_shape=jax.ShapeDtypeStruct((C, D), BF16)...  103 us

profile of v1, /device:TPU:1, one launch (start us, length us, event | category | flops | bytes accessed | tf_op | source)
XLA Modules:
  0.0 104.9 jit_solution(1543923650491706699)
XLA Ops:
  0.0 103.0 %layer.1 = bf16[128,2048]{1,0:T(8,128)(2,1)} custom-call(bf16[128,1024]{1,0:T(8,128)(2,1)} %bitcast.32, bf16[128,1024]{1,0:T(8,128)(2,1)} %bitcast.33, bf16[128,2048]{1,0:T(8,128)(2,1)} %bitcast.29, bf16[128,2048]{1,0:T(8,128)(2,1)} %bitcast.30, bf16[128,2048]{1,0:T(8,128)(2,1)} %bitcast.31, bf16[2048,256]{1,0:T(8,128)(2,1)} %wo_hbm.1, ...), custom_call_target="tpu_custom_call" | custom-call | tf_op jit(solution)/shard_map/layer/pallas_call | solution.py:467
  103.0 1.9 %copy.20 = bf16[1,128,2048]{2,1,0:T(8,128)(2,1)} copy(bf16[1,128,2048]{2,1,0:T(8,128)(2,1)} %bitcast.28) | data formatting | bytes 1048576

commit v2 on v1

--- a/solution.py
+++ b/solution.py
@@ -21,7 +21,9 @@
 PER = DEVICES // CHUNKS
 PAIRS = H // 2
 STRIDE = 11
-QUARTER = D // 4
+PIECE = 32
+BASE = H * PIECE
+QUARTER = (D - BASE) // 4
 NT = (((1,), (1,)), ((), ()))
 TN = (((0,), (0,)), ((), ()))
 MESH = pl.DeviceIdType.MESH
@@ -33,14 +35,15 @@
 
 def layer_kernel(
     q_hbm, k_hbm, v_hbm, ogl_hbm, res_hbm, wo_hbm, gate_hbm, up_hbm, down_hbm,
+    g_hbm, ext_hbm, lam_hbm, ro_hbm, ids_hbm, group_hbm, within_hbm, cng_hbm, eng_hbm,
+    out_ref,
     g_ref, ext_ref, lam_ref, ro_ref, ids_ref, group_ref, within_ref, cng_ref, eng_ref,
-    out_ref,
     q_ref, k_ref, v_ref, ogl_ref, res_ref, wbuf, gate_w, up_w, down_w,
     msg, rx1, lst, lsm, rxs, rxm, ent, enm, est, esm,
-    gates, fcol, bcol, rows, nfb, zfb, sg,
+    gates, fcol, bcol, rows, wpair, nfb, zfb, sg,
     gated, proj, tab_send, tab_back, outgoing, arrived, produced, returned,
-    loc, sa, ra, sb, rb, sc, rc, sd, rd, se, re,
-    wsr, wsl, wrl, wrr, wps, wpr, ds, dr, bs, br,
+    loc, sa, ra, sb, rb, sbb, rbb, sc, rc, sd, rd, se, re, seb, reb,
+    wsr, wsl, wrl, wrr, wps, wpr, pxs, pxr, pys, pyr, ds, dr, bs, br, meet,
 ):
     me = lax.axis_index("sp")
     dp = lax.axis_index("dp")
@@ -67,24 +70,27 @@
 
         lax.fori_loop(1, H, step, 0)
 
+    barrier = pltpu.get_barrier_semaphore()
+
+    def greet(where):
+        pl.semaphore_signal(barrier, inc=1, device_id=where, device_id_type=MESH)
+
+    each_peer(lambda p: greet((p, dp)))
+    for n in range(1, 8):
+        greet((me, lax.rem(dp + n, 8)))
+
     local = [
         pltpu.make_async_copy(src, dst, loc.at[i])
         for i, (src, dst) in enumerate((
-            (wo_hbm, wbuf.at[dp]), (k_hbm, k_ref), (v_hbm, v_ref), (ogl_hbm, ogl_ref), (q_hbm, q_ref),
+            (ext_hbm, ext_ref), (lam_hbm, lam_ref), (ro_hbm, ro_ref), (g_hbm, g_ref),
+            (wo_hbm, wbuf.at[dp]), (k_hbm, k_ref), (v_hbm, v_ref), (q_hbm, q_ref), (ogl_hbm, ogl_ref),
+            (ids_hbm, ids_ref), (group_hbm, group_ref), (within_hbm, within_ref),
+            (cng_hbm, cng_ref), (eng_hbm, eng_ref),
             (res_hbm, res_ref), (gate_hbm, gate_w), (up_hbm, up_w), (down_hbm, down_w),
         ))
     ]
-    for c in local[:5]:
+    for c in local[:14]:
         c.start()
-
-    barrier = pltpu.get_barrier_semaphore()
-
-    def greet(d, carry):
-        other = lax.rem(flat + d, DEVICES)
-        pl.semaphore_signal(barrier, inc=1, device_id=(lax.div(other, 8), lax.rem(other, 8)), device_id_type=MESH)
-        return carry
-
-    lax.fori_loop(1, DEVICES, greet, 0)
 
     lane = lax.broadcasted_iota(jnp.int32, (C, C), 1)
     row_id = lax.broadcasted_iota(jnp.int32, (C, C), 0)
@@ -93,6 +99,8 @@
     earlier = lane <= row_id
     diagonal = lane == row_id
 
+    for c in local[:4]:
+        c.wait()
     msg[:, 0, :] = ext_ref[...]
     msg[:, 1, :] = jnp.broadcast_to(lam_ref[...], (H, C))
     msg[:, 2, :] = jnp.broadcast_to(ro_ref[:, 0:1], (H, C))
@@ -100,9 +108,7 @@
     for i in range(4, 8):
         msg[:, i, :] = jnp.zeros((H, C), F32)
     gates[...] = g_ref[...].astype(F32)
-    for c in local[:5]:
-        c.wait()
-    pl.semaphore_wait(barrier, DEVICES - 1)
+    pl.semaphore_wait(barrier, H - 1 + 7)
 
     each_peer(lambda p: remote(msg.at[p], rx1.at[me], sa.at[p], ra.at[me], p).start())
     rx1[me] = msg[me]
@@ -113,7 +119,28 @@
     partner = x * 2 + 1 - core
 
     def piece(shard, i):
-        return wbuf.at[shard, pl.ds(i * QUARTER, QUARTER), :]
+        return wbuf.at[shard, pl.ds(BASE + i * QUARTER, QUARTER), :]
+
+    def strip(shard, owner):
+        return wbuf.at[shard, pl.ds(pl.multiple_of(owner * PIECE, PIECE), PIECE), :]
+
+    others = ((right, left), (left, right), (across, across))
+
+    def strip_out(n):
+        ref = strip(dp, me)
+        return copy_to(ref, ref, pxs.at[n], pxr.at[n], (me, others[n][0]))
+
+    def strip_on(n, peer):
+        ref = strip(others[n][1], me)
+        return copy_to(ref, ref, pys.at[n], pyr.at[n], (peer, dp))
+
+    def strips(n):
+        ref = wbuf.at[others[n][1], pl.ds(0, BASE - PIECE), :]
+        return copy_to(ref, ref, pys.at[n], pyr.at[n], (me, partner))
+
+    def pass_strip(n):
+        strip_out(n).wait_recv()
+        each_peer(lambda p: strip_on(n, p).start())
 
     def to_right(shard, i, n):
         return copy_to(piece(shard, i), piece(shard, i), wsr.at[n], wrl.at[n], (me, right))
@@ -124,11 +151,16 @@
     def to_partner(ref, n):
         return copy_to(ref, ref, wps.at[n], wpr.at[n], (me, partner))
 
+    local[4].wait()
+    for n in range(3):
+        strip_out(n).start()
     for n in range(4):
         to_right(dp, n, n).start()
         to_left(dp, (n + 2) % 4, n).start()
     to_partner(wbuf.at[dp], 0).start()
-    for c in local[5:]:
+    for c in local[5:14]:
+        c.wait()
+    for c in local[14:]:
         c.start()
 
     def gate_step(p, carry):
@@ -138,125 +170,7 @@
 
     lax.fori_loop(0, PAIRS, gate_step, 0)
 
-    each_peer(lambda p: remote(msg.at[p], rx1.at[p], sa.at[p], ra.at[p], p).wait_recv())
-
-    spread = rx1[:, 0, :]
-    in_f = gates[pl.ds(0, H, stride=4), :]
-    in_b = gates[pl.ds(2, H, stride=4), :]
-    fade_f = log_sigmoid(gates[pl.ds(1, H, stride=4), :] + rx1[:, 2, :]) + spread
-    fade_b = log_sigmoid(gates[pl.ds(3, H, stride=4), :] + rx1[:, 3, :]) + spread
-    upto = (row_id <= lane).astype(F32)
-    since = (row_id >= lane).astype(F32)
-    cum_f = jnp.dot(fade_f, upto, precision=HIGH, preferred_element_type=F32)
-    cum_b = jnp.dot(fade_b, since, precision=HIGH, preferred_element_type=F32)
-    end_f = jnp.broadcast_to(cum_f[:, C - 1:C], (H, C))
-    end_b = jnp.broadcast_to(cum_b[:, 0:1], (H, C))
-    w_f = jnp.exp(end_f - cum_f + in_f)
-    w_b = jnp.exp(end_b - cum_b + in_b)
-    rows[0] = cum_f - in_f
-    rows[1] = cum_b - in_b
-    rows[2] = jnp.exp(in_b)
-    turned = jnp.concatenate([cum_f, cum_b, w_f, w_b, jnp.zeros((C - 4 * H, C), F32)], axis=0).T
-    wf_hi = w_f.astype(BF16)
-    wb_hi = w_b.astype(BF16)
-    wf_lo = (w_f - wf_hi.astype(F32)).astype(BF16)
-    wb_lo = (w_b - wb_hi.astype(F32)).astype(BF16)
-    stacked = jnp.concatenate([wf_hi, wf_lo, wb_hi, wb_lo], axis=0)
-    for p in range(PAIRS):
-        kp = k_ref[:, p * C:(p + 1) * C]
-        k32 = kp.astype(F32)
-        h0, h1 = 2 * p, 2 * p + 1
-        wf = jnp.where(low_half, turned[:, 32 + h0:33 + h0], turned[:, 32 + h1:33 + h1])
-        wb = jnp.where(low_half, turned[:, 48 + h0:49 + h0], turned[:, 48 + h1:49 + h1])
-        both = jnp.concatenate([k32 * wf, k32 * wb], axis=1).astype(BF16)
-        state = lax.dot_general(both, v_ref[:, p * 256:(p + 1) * 256], TN, preferred_element_type=F32).astype(BF16)
-        lst[h0, 0] = state[0:64, 0:128]
-        lst[h1, 0] = state[64:128, 128:256]
-        lst[h0, 1] = state[128:192, 0:128]
-        lst[h1, 1] = state[192:256, 128:256]
-        norm = jnp.dot(stacked, kp, preferred_element_type=F32)
-        norm_f = norm[0:16] + norm[16:32]
-        norm_b = norm[32:48] + norm[48:64]
-        for h, keep in ((h0, low_row), (h1, ~low_row)):
-            nf = norm_f[h:h + 1]
-            nb = norm_b[h:h + 1]
-            nf = jnp.where(keep, nf, pltpu.roll(nf, DK, 1))
-            nb = jnp.where(keep, nb, pltpu.roll(nb, DK, 1))
-            lsm[h] = jnp.concatenate(
-                [nf, nb, end_f[h:h + 1], end_b[h:h + 1], jnp.zeros((4, C), F32)], axis=0)
-
-    each_peer(lambda p: remote(lsm.at[p], rxm.at[me], sc.at[p], rc.at[me], p).start())
-    each_peer(lambda p: remote(lst.at[p], rxs.at[me], sb.at[p], rb.at[me], p).start())
-    rxs[me] = lst[me]
-    rxm[me] = lsm[me]
-
-    for h in range(H):
-        fcol[h] = jnp.broadcast_to(turned[:, h:h + 1], (C, C))
-        bcol[h] = jnp.broadcast_to(turned[:, 16 + h:17 + h], (C, C))
-
-    def lhs_of(cols):
-        qp = q_ref[:, cols] * jnp.asarray(DK ** -0.5, BF16)
-        none = jnp.zeros_like(qp)
-        return jnp.concatenate([jnp.where(low_half, qp, none), jnp.where(low_half, none, qp)], axis=0)
-
-    def inner_step(p, carry):
-        cols = pl.ds(pl.multiple_of(p * C, C), C)
-        score2 = lax.dot_general(lhs_of(cols), k_ref[:, cols], NT, preferred_element_type=F32)
-        for hh in range(2):
-            h = 2 * p + hh
-            score = score2[hh * C:(hh + 1) * C]
-            ahead = fcol[h] - rows[0, pl.ds(h, 1), :]
-            behind = bcol[h] - rows[1, pl.ds(h, 1), :]
-            weighted = score * jnp.exp(jnp.where(earlier, ahead, behind))
-            pf = jnp.where(earlier, weighted, 0.0)
-            pb = jnp.where(earlier, jnp.where(diagonal, score * rows[2, pl.ds(h, 1), :], 0.0), weighted)
-            both = jnp.concatenate([pf, pb], axis=0)
-            zfb[h] = jnp.broadcast_to(jnp.sum(both, axis=1, keepdims=True), (2 * C, C))
-            vcols = pl.ds(pl.multiple_of(h * DV, DV), DV)
-            nfb[h] = jnp.dot(both.astype(BF16), v_ref[:, vcols], preferred_element_type=F32)
-        return carry
-
-    lax.fori_loop(0, PAIRS, inner_step, 0)
-
-    each_peer(lambda p: remote(lsm.at[p], rxm.at[p], sc.at[p], rc.at[p], p).wait_recv())
-    each_peer(lambda p: remote(lst.at[p], rxs.at[p], sb.at[p], rb.at[p], p).wait_recv())
-
-    enm[...] = jnp.zeros_like(enm)
-
-    def carry_step(c, state):
-        mf, mb, nf, nb = state
-        d = H - 1 - c
-        ent[c, 0] = mf.astype(BF16)
-        ent[d, 1] = mb.astype(BF16)
-        enm[c, 0:1] = nf
-        enm[d, 1:2] = nb
-        keep_f = jnp.exp(rxm[c, 2:3])
-        keep_b = jnp.exp(rxm[d, 3:4])
-        return (
-            mf * keep_f + rxs[c, 0].astype(F32),
-            mb * keep_b + rxs[d, 1].astype(F32),
-            nf * keep_f + rxm[c, 0:1],
-            nb * keep_b + rxm[d, 1:2],
-        )
-
-    zero_m = jnp.zeros((DK, DV), F32)
-    zero_n = jnp.zeros((1, C), F32)
-    lax.fori_loop(0, H, carry_step, (zero_m, zero_m, zero_n, zero_n))
-
-    def slot(h):
-        return est.at[lax.div(h, 2), :, pl.ds(pl.multiple_of(lax.rem(h, 2) * DK, DK), DK), :]
-
-    each_peer(lambda p: remote(enm.at[p], esm.at[me], sd.at[p], rd.at[me], p).start())
-    each_peer(lambda p: remote(ent.at[p], slot(me), se.at[p], re.at[me], p).start())
-    esm[me] = enm[me]
-    est[lax.div(me, 2), :, pl.ds(pl.multiple_of(lax.rem(me, 2) * DK, DK), DK), :] = ent[me]
-
-    for n in range(2):
-        to_right(left, n, n).wait_recv()
-        to_right(left, n, 4 + n).start()
-        to_left(right, n + 2, n).wait_recv()
-        to_left(right, n + 2, 4 + n).start()
-
+    pass_strip(0)
     table_in = jnp.concatenate(
         [ids_ref[...].astype(F32), group_ref[...], within_ref[...], jnp.zeros((C - 8, C), F32)], axis=0).T
     wide = lax.broadcasted_iota(jnp.int32, (C, DEVICES * CAP), 1)
@@ -288,14 +202,169 @@
     tab_back[0:C] = back_hi
     tab_back[C:2 * C] = (back - back_hi.astype(F32)).astype(BF16)
 
-    def outer_step(p, carry):
+    each_peer(lambda p: remote(msg.at[p], rx1.at[p], sa.at[p], ra.at[p], p).wait_recv())
+
+    spread = rx1[:, 0, :]
+    in_f = gates[pl.ds(0, H, stride=4), :]
+    in_b = gates[pl.ds(2, H, stride=4), :]
+    fade_f = log_sigmoid(gates[pl.ds(1, H, stride=4), :] + rx1[:, 2, :]) + spread
+    fade_b = log_sigmoid(gates[pl.ds(3, H, stride=4), :] + rx1[:, 3, :]) + spread
+    upto = (row_id <= lane).astype(F32)
+    since = (row_id >= lane).astype(F32)
+    cum_f = jnp.dot(fade_f, upto, precision=HIGH, preferred_element_type=F32)
+    cum_b = jnp.dot(fade_b, since, precision=HIGH, preferred_element_type=F32)
+    end_f = jnp.broadcast_to(cum_f[:, C - 1:C], (H, C))
+    end_b = jnp.broadcast_to(cum_b[:, 0:1], (H, C))
+    w_f = jnp.exp(end_f - cum_f + in_f)
+    w_b = jnp.exp(end_b - cum_b + in_b)
+    rows[0] = cum_f - in_f
+    rows[1] = cum_b - in_b
+    rows[2] = jnp.exp(in_b)
+    turned = jnp.concatenate([cum_f, cum_b, w_f, w_b, jnp.zeros((C - 4 * H, C), F32)], axis=0).T
+    wf_hi = w_f.astype(BF16)
+    wb_hi = w_b.astype(BF16)
+    wf_lo = (w_f - wf_hi.astype(F32)).astype(BF16)
+    wb_lo = (w_b - wb_hi.astype(F32)).astype(BF16)
+    stacked = jnp.concatenate([wf_hi, wf_lo, wb_hi, wb_lo], axis=0)
+    norm = jnp.dot(stacked, k_ref[...], preferred_element_type=F32)
+    norm_f = norm[0:16] + norm[16:32]
+    norm_b = norm[32:48] + norm[48:64]
+    for p in range(PAIRS):
+        h0, h1 = 2 * p, 2 * p + 1
+        wpair[p, 0] = jnp.where(low_half, turned[:, 32 + h0:33 + h0], turned[:, 32 + h1:33 + h1])
+        wpair[p, 1] = jnp.where(low_half, turned[:, 48 + h0:49 + h0], turned[:, 48 + h1:49 + h1])
+        for h, keep in ((h0, low_row), (h1, ~low_row)):
+            nf = norm_f[h:h + 1, p * C:(p + 1) * C]
+            nb = norm_b[h:h + 1, p * C:(p + 1) * C]
+            nf = jnp.where(keep, nf, pltpu.roll(nf, DK, 1))
+            nb = jnp.where(keep, nb, pltpu.roll(nb, DK, 1))
+            lsm[h] = jnp.concatenate(
+                [nf, nb, end_f[h:h + 1], end_b[h:h + 1], jnp.zeros((4, C), F32)], axis=0)
+
+    each_peer(lambda p: remote(lsm.at[p], rxm.at[me], sc.at[p], rc.at[me], p).start())
+    rxm[me] = lsm[me]
+    first = lax.div(me, 2) + 1
+
+    def state_out(way, h, ssem, rsem):
+        return remote(lst.at[h, way], rxs.at[me, way], ssem.at[h], rsem.at[me], h)
+
+    def state_in(way, h, ssem, rsem):
+        return remote(lst.at[h, way], rxs.at[h, way], ssem.at[h], rsem.at[h], h)
+
+    def post_pair(i):
+        p = lax.rem(first + i, PAIRS)
+        for hh in range(2):
+            h = 2 * p + hh
+
+            @pl.when(h != me)
+            def _():
+                state_out(0, h, sb, rb).start()
+
+    def state_step(i, carry):
+        p = lax.rem(first + i, PAIRS)
+        k32 = k_ref[:, pl.ds(pl.multiple_of(p * C, C), C)].astype(F32)
+        both = jnp.concatenate([k32 * wpair[p, 0], k32 * wpair[p, 1]], axis=1).astype(BF16)
+        vp = v_ref[:, pl.ds(pl.multiple_of(p * 256, 256), 256)]
+        state = lax.dot_general(both, vp, TN, preferred_element_type=F32).astype(BF16)
+        lst[2 * p, 0] = state[0:64, 0:128]
+        lst[2 * p + 1, 0] = state[64:128, 128:256]
+        lst[2 * p, 1] = state[128:192, 0:128]
+        lst[2 * p + 1, 1] = state[192:256, 128:256]
+
+        @pl.when(i > 0)
+        def _():
+            post_pair(i - 1)
+
+        return carry
+
+    lax.fori_loop(0, PAIRS, state_step, 0)
+    post_pair(PAIRS - 1)
+    each_peer(lambda p: state_out(1, p, sbb, rbb).start())
+    rxs[me] = lst[me]
+
+    def relay(n):
+        to_right(left, n, n).wait_recv()
+        to_right(left, n, 4 + n).start()
+        to_left(right, n + 2, n).wait_recv()
+        to_left(right, n + 2, 4 + n).start()
+
+
+    for h in range(H):
+        fcol[h] = jnp.broadcast_to(turned[:, h:h + 1], (C, C))
+        bcol[h] = jnp.broadcast_to(turned[:, 16 + h:17 + h], (C, C))
+
+    relay(0)
+
+    def lhs_of(cols):
+        qp = q_ref[:, cols] * jnp.asarray(DK ** -0.5, BF16)
+        none = jnp.zeros_like(qp)
+        return jnp.concatenate([jnp.where(low_half, qp, none), jnp.where(low_half, none, qp)], axis=0)
+
+    def inner_step(p, carry):
+        cols = pl.ds(pl.multiple_of(p * C, C), C)
+        score2 = lax.dot_general(lhs_of(cols), k_ref[:, cols], NT, preferred_element_type=F32)
+        for hh in range(2):
+            h = 2 * p + hh
+            score = score2[hh * C:(hh + 1) * C]
+            ahead = fcol[h] - rows[0, pl.ds(h, 1), :]
+            behind = bcol[h] - rows[1, pl.ds(h, 1), :]
+            weighted = score * jnp.exp(jnp.where(earlier, ahead, behind))
+            pf = jnp.where(earlier, weighted, 0.0)
+            pb = jnp.where(earlier, jnp.where(diagonal, score * rows[2, pl.ds(h, 1), :], 0.0), weighted)
+            both = jnp.concatenate([pf, pb], axis=0)
+            zfb[h] = jnp.broadcast_to(jnp.sum(both, axis=1, keepdims=True), (2 * C, C))
+            vcols = pl.ds(pl.multiple_of(h * DV, DV), DV)
+            nfb[h] = jnp.dot(both.astype(BF16), v_ref[:, vcols], preferred_element_type=F32)
+        return carry
+
+    lax.fori_loop(0, PAIRS, inner_step, 0)
+
+    relay(1)
+    each_peer(lambda p: remote(lsm.at[p], rxm.at[p], sc.at[p], rc.at[p], p).wait_recv())
+    enm[...] = jnp.zeros_like(enm)
+
+    def slot(way, h):
+        return est.at[lax.div(h, 2), way, pl.ds(pl.multiple_of(lax.rem(h, 2) * DK, DK), DK), :]
+
+    def entry_out(way, p, ssem, rsem):
+        return remote(ent.at[p, way], slot(way, me), ssem.at[p], rsem.at[me], p)
+
+    def entry_in(way, p, ssem, rsem):
+        return remote(ent.at[p, way], slot(way, p), ssem.at[p], rsem.at[p], p)
+
+    def run(way, ssem, rsem, ssem_out, rsem_out):
+        each_peer(lambda p: state_in(way, p, ssem, rsem).wait_recv())
+
+        def carry_step(i, state):
+            m, n = state
+            c = i if way == 0 else H - 1 - i
+            ent[c, way] = m.astype(BF16)
+            enm[c, way:way + 1] = n
+            keep = jnp.exp(rxm[c, 2 + way:3 + way])
+            return m * keep + rxs[c, way].astype(F32), n * keep + rxm[c, way:way + 1]
+
+        lax.fori_loop(0, H, carry_step, (jnp.zeros((DK, DV), F32), jnp.zeros((1, C), F32)))
+        each_peer(lambda p: entry_out(way, p, ssem_out, rsem_out).start())
+
+    run(0, sb, rb, se, re)
+    run(1, sbb, rbb, seb, reb)
+    each_peer(lambda p: remote(enm.at[p], esm.at[me], sd.at[p], rd.at[me], p).start())
+    esm[me] = enm[me]
+    est[lax.div(me, 2), :, pl.ds(pl.multiple_of(lax.rem(me, 2) * DK, DK), DK), :] = ent[me]
+    pass_strip(1)
+    pass_strip(2)
+
+
+    def outer_step(i, carry):
+        p = lax.rem(lax.div(me, 2) + PAIRS - i, PAIRS)
         for hh in range(2):
             h = 2 * p + hh
 
             @pl.when(h != me)
             def _():
                 remote(enm.at[h], esm.at[h], sd.at[h], rd.at[h], h).wait_recv()
-                remote(ent.at[h], slot(h), se.at[h], re.at[h], h).wait_recv()
+                entry_in(0, h, se, re).wait_recv()
+                entry_in(1, h, seb, reb).wait_recv()
 
         cols = pl.ds(pl.multiple_of(p * C, C), C)
         lhs = lhs_of(cols)
@@ -327,33 +396,42 @@
         cols = pl.ds(pl.multiple_of(shard * 256, 256), 256)
         proj[:, cols] = jnp.dot(gated[...], wbuf[shard], preferred_element_type=F32)
 
+    for n in range(1, 8):
+        pl.semaphore_signal(meet, inc=1, device_id=(me, lax.rem(dp + n, 8)), device_id_type=MESH)
+    each_peer(lambda p: pl.semaphore_signal(meet, inc=1, device_id=(p, dp), device_id_type=MESH))
     project(dp)
     for n in range(2, 4):
         to_right(left, n, n).wait_recv()
         to_left(right, n - 2, n).wait_recv()
+    strips(0).wait_recv()
     to_partner(wbuf.at[left], 1).start()
+    project(left)
+    strips(1).wait_recv()
     to_partner(wbuf.at[right], 2).start()
-    project(left)
     project(right)
+    strips(2).wait_recv()
+    edge = pl.ds(0, BASE)
+    to_partner(wbuf.at[across, edge, :], 3).start()
     far = 1 - 2 * core
     to_partner(wbuf.at[partner], 0).wait_recv()
     project(partner)
     for n in range(2):
         to_right(across, n, 4 + n).wait_recv()
-        to_partner(piece(across, n), 3 + n).start()
+        to_partner(piece(across, n), 4 + n).start()
         to_left(across, n + 2, 4 + n).wait_recv()
-        to_partner(piece(across, n + 2), 5 + n).start()
+        to_partner(piece(across, n + 2), 6 + n).start()
     to_partner(wbuf.at[left + far], 1).wait_recv()
     project(left + far)
     to_partner(wbuf.at[right + far], 2).wait_recv()
     project(right + far)
     project(across)
+    to_partner(wbuf.at[across + far, edge, :], 3).wait_recv()
     for n in range(2):
-        to_partner(piece(across + far, n), 3 + n).wait_recv()
-        to_partner(piece(across + far, n + 2), 5 + n).wait_recv()
+        to_partner(piece(across + far, n), 4 + n).wait_recv()
+        to_partner(piece(across + far, n + 2), 6 + n).wait_recv()
     project(across + far)
 
-    local[5].wait()
+    local[14].wait()
     pr = proj[...]
     scale = lax.rsqrt(jnp.mean(pr * pr, axis=1, keepdims=True) + EPS)
     stream = (res_ref[...].astype(F32) + cng_ref[...] * pr * scale).astype(BF16).astype(F32)
@@ -401,11 +479,13 @@
         rows_out = lax.dot_general(
             tab_send[:, j * C:(j + 1) * C], gated[...], TN, preferred_element_type=F32)
         outgoing[j * PER:(j + 1) * PER] = rows_out.astype(BF16).reshape(PER, CAP, D)
+        if j == 0:
+            pl.semaphore_wait(meet, H - 1 + 7)
         send_chunk(j, onward, outgoing, arrived, ds, dr)
         if j == 0:
             arrived[0] = outgoing[0]
 
-    for c in local[6:]:
+    for c in local[15:]:
         c.wait()
 
     def expert_chunk(j):
@@ -422,11 +502,16 @@
             def _():
                 whole(n, outgoing, arrived, ds, dr).wait_recv()
 
+        @pl.when(j >= 1)
+        def _():
+            send_chunk(j - 1, homeward, produced, returned, bs, br)
+
         expert_chunk(j)
+        return carry
+
+    lax.fori_loop(0, CHUNKS, expert_step, 0)
+    for j in range(CHUNKS - 1, CHUNKS):
         send_chunk(j, homeward, produced, returned, bs, br)
-        return carry
-
-    lax.fori_loop(0, CHUNKS, expert_step, 0)
     returned[0] = produced[0]
 
     for j in range(CHUNKS):
@@ -438,16 +523,22 @@
 
     each_peer(lambda p: remote(msg.at[p], rx1.at[me], sa.at[p], ra.at[me], p).wait_send())
     each_peer(lambda p: remote(lsm.at[p], rxm.at[me], sc.at[p], rc.at[me], p).wait_send())
-    each_peer(lambda p: remote(lst.at[p], rxs.at[me], sb.at[p], rb.at[me], p).wait_send())
+    each_peer(lambda p: state_out(0, p, sb, rb).wait_send())
+    each_peer(lambda p: state_out(1, p, sbb, rbb).wait_send())
     each_peer(lambda p: remote(enm.at[p], esm.at[me], sd.at[p], rd.at[me], p).wait_send())
-    each_peer(lambda p: remote(ent.at[p], slot(me), se.at[p], re.at[me], p).wait_send())
+    each_peer(lambda p: entry_out(0, p, se, re).wait_send())
+    each_peer(lambda p: entry_out(1, p, seb, reb).wait_send())
     for n in range(6):
         to_right(dp, 0, n).wait_send()
         to_left(dp, 0, n).wait_send()
     for n in range(3):
         to_partner(wbuf.at[dp], n).wait_send()
-    for n in range(3, 7):
+    to_partner(wbuf.at[dp, edge, :], 3).wait_send()
+    for n in range(4, 8):
         to_partner(piece(dp, 0), n).wait_send()
+    for n in range(3):
+        strip_out(n).wait_send()
+        strips(n).wait_send()
     for j in range(CHUNKS):
         whole(j, outgoing, arrived, ds, dr).wait_send()
         whole(j, produced, returned, bs, br).wait_send()
@@ -467,9 +558,18 @@
     out = pl.pallas_call(
         layer_kernel,
         out_shape=jax.ShapeDtypeStruct((C, D), BF16),
-        in_specs=[hbm] * 9 + [vm] * 9,
+        in_specs=[hbm] * 18,
         out_specs=vm,
         scratch_shapes=[
+            pltpu.VMEM((4 * H, C), BF16),
+            pltpu.VMEM((H, C), F32),
+            pltpu.VMEM((1, C), F32),
+            pltpu.VMEM((1, 2), F32),
+            pltpu.VMEM((2, C), jnp.int32),
+            pltpu.VMEM((4, C), F32),
+            pltpu.VMEM((2, C), F32),
+            pltpu.VMEM((1, D), F32),
+            pltpu.VMEM((1, D), F32),
             pltpu.VMEM((C, H * DK), BF16),
             pltpu.VMEM((C, H * DK), BF16),
             pltpu.VMEM((C, H * DV), BF16),
@@ -486,6 +586,7 @@
             pltpu.VMEM((H, C, C), F32),
             pltpu.VMEM((H, C, C), F32),
             pltpu.VMEM((3, H, C), F32),
+            pltpu.VMEM((PAIRS, 2, C, C), F32),
             pltpu.VMEM((H, 2 * C, DV), F32),
             pltpu.VMEM((H, 2 * C, C), F32),
             pltpu.VMEM((C, H * DV), F32),
@@ -494,8 +595,8 @@
             pltpu.VMEM((C, DEVICES * CAP), BF16),
             pltpu.VMEM((2 * C, DEVICES * CAP), BF16),
             slots, slots, slots, slots,
-            dma((9,)),
-        ] + [dma((H,))] * 10 + [dma((6,))] * 4 + [dma((7,))] * 2 + [dma((CHUNKS,))] * 4,
+            dma((18,)),
+        ] + [dma((H,))] * 14 + [dma((6,))] * 4 + [dma((8,))] * 2 + [dma((3,))] * 4 + [dma((CHUNKS,))] * 4 + [pltpu.SemaphoreType.REGULAR],
         compiler_params=pltpu.CompilerParams(
             collective_id=0, has_side_effects=True, vmem_limit_bytes=67_043_328),
         name="layer",

time: 105 us -> 96 us (0.914)
  Pallas kernels: 103 us -> 94 us
    pallas_call x1, Pallas kernels: 103 us -> 94 us  [on_device(): pl.pallas_call(layer_kernel, out_shape=jax.ShapeDtypeStruct((C, D), BF16)...]
where the time goes in v2:
time: 96 us; the launch traced here: 95.9 us
  Pallas kernels  94 us (98%)
  local copies, waits for them, and re-layouts  1.88 us (2%)
    pallas_call x1, Pallas kernels, on_device(): pl.pallas_call(layer_kernel, out_shape=jax.ShapeDtypeStruct((C, D), BF16)...  94 us

profile of v2, /device:TPU:1, one launch (start us, length us, event | category | flops | bytes accessed | tf_op | source)
XLA Modules:
  0.0 95.9 jit_solution(14655854961184556752)
XLA Ops:
  0.0 94.0 %layer.1 = bf16[128,2048]{1,0:T(8,128)(2,1)} custom-call(bf16[128,1024]{1,0:T(8,128)(2,1)} %bitcast.32, bf16[128,1024]{1,0:T(8,128)(2,1)} %bitcast.33, bf16[128,2048]{1,0:T(8,128)(2,1)} %bitcast.29, bf16[128,2048]{1,0:T(8,128)(2,1)} %bitcast.30, bf16[128,2048]{1,0:T(8,128)(2,1)} %bitcast.31, bf16[2048,256]{1,0:T(8,128)(2,1)} %wo_hbm.1, ...), custom_call_target="tpu_custom_call" | custom-call | tf_op jit(solution)/shard_map/layer/pallas_call | solution.py:558
  94.0 1.9 %copy.20 = bf16[1,128,2048]{2,1,0:T(8,128)(2,1)} copy(bf16[1,128,2048]{2,1,0:T(8,128)(2,1)} %bitcast.28) | data formatting | bytes 1048576

commit v3 on v2

--- a/solution.py
+++ b/solution.py
@@ -20,7 +20,7 @@
 CHUNKS = 4
 PER = DEVICES // CHUNKS
 PAIRS = H // 2
-STRIDE = 11
+STRIDE = 7
 PIECE = 32
 BASE = H * PIECE
 QUARTER = (D - BASE) // 4
@@ -63,6 +63,10 @@
     def remote(src, dst, ssem, rsem, peer):
         return copy_to(src, dst, ssem, rsem, (peer, dp))
 
+    def fifteen(src, dst, ssem, rsem):
+        most = pl.ds(0, H - 1)
+        return remote(src.at[most], dst.at[most], ssem.at[0], rsem.at[0], peer_of(1))
+
     def each_peer(body):
         def step(d, carry):
             body(peer_of(d))
@@ -110,7 +114,7 @@
     gates[...] = g_ref[...].astype(F32)
     pl.semaphore_wait(barrier, H - 1 + 7)
 
-    each_peer(lambda p: remote(msg.at[p], rx1.at[me], sa.at[p], ra.at[me], p).start())
+    each_peer(lambda p: remote(msg.at[p], rx1.at[me], sa.at[0], ra.at[0], p).start())
     rx1[me] = msg[me]
 
     right = lax.rem(x + 1, 4) * 2 + core
@@ -202,7 +206,7 @@
     tab_back[0:C] = back_hi
     tab_back[C:2 * C] = (back - back_hi.astype(F32)).astype(BF16)
 
-    each_peer(lambda p: remote(msg.at[p], rx1.at[p], sa.at[p], ra.at[p], p).wait_recv())
+    fifteen(msg, rx1, sa, ra).wait_recv()
 
     spread = rx1[:, 0, :]
     in_f = gates[pl.ds(0, H, stride=4), :]
@@ -241,15 +245,16 @@
             lsm[h] = jnp.concatenate(
                 [nf, nb, end_f[h:h + 1], end_b[h:h + 1], jnp.zeros((4, C), F32)], axis=0)
 
-    each_peer(lambda p: remote(lsm.at[p], rxm.at[me], sc.at[p], rc.at[me], p).start())
+    each_peer(lambda p: remote(lsm.at[p], rxm.at[me], sc.at[0], rc.at[0], p).start())
     rxm[me] = lsm[me]
     first = lax.div(me, 2) + 1
 
     def state_out(way, h, ssem, rsem):
-        return remote(lst.at[h, way], rxs.at[me, way], ssem.at[h], rsem.at[me], h)
-
-    def state_in(way, h, ssem, rsem):
-        return remote(lst.at[h, way], rxs.at[h, way], ssem.at[h], rsem.at[h], h)
+        return remote(lst.at[h, way], rxs.at[me, way], ssem.at[0], rsem.at[0], h)
+
+    def states_in(way, ssem, rsem):
+        most = pl.ds(0, H - 1)
+        return remote(lst.at[most, way], rxs.at[most, way], ssem.at[0], rsem.at[0], peer_of(1))
 
     def post_pair(i):
         p = lax.rem(first + i, PAIRS)
@@ -320,20 +325,20 @@
     lax.fori_loop(0, PAIRS, inner_step, 0)
 
     relay(1)
-    each_peer(lambda p: remote(lsm.at[p], rxm.at[p], sc.at[p], rc.at[p], p).wait_recv())
+    fifteen(lsm, rxm, sc, rc).wait_recv()
     enm[...] = jnp.zeros_like(enm)
 
     def slot(way, h):
         return est.at[lax.div(h, 2), way, pl.ds(pl.multiple_of(lax.rem(h, 2) * DK, DK), DK), :]
 
     def entry_out(way, p, ssem, rsem):
-        return remote(ent.at[p, way], slot(way, me), ssem.at[p], rsem.at[me], p)
+        return remote(ent.at[p, way], slot(way, me), ssem.at[0], rsem.at[me], p)
 
     def entry_in(way, p, ssem, rsem):
-        return remote(ent.at[p, way], slot(way, p), ssem.at[p], rsem.at[p], p)
+        return remote(ent.at[p, way], slot(way, p), ssem.at[0], rsem.at[p], p)
 
     def run(way, ssem, rsem, ssem_out, rsem_out):
-        each_peer(lambda p: state_in(way, p, ssem, rsem).wait_recv())
+        states_in(way, ssem, rsem).wait_recv()
 
         def carry_step(i, state):
             m, n = state
@@ -348,7 +353,7 @@
 
     run(0, sb, rb, se, re)
     run(1, sbb, rbb, seb, reb)
-    each_peer(lambda p: remote(enm.at[p], esm.at[me], sd.at[p], rd.at[me], p).start())
+    each_peer(lambda p: remote(enm.at[p], esm.at[me], sd.at[0], rd.at[me], p).start())
     esm[me] = enm[me]
     est[lax.div(me, 2), :, pl.ds(pl.multiple_of(lax.rem(me, 2) * DK, DK), DK), :] = ent[me]
     pass_strip(1)
@@ -362,7 +367,7 @@
 
             @pl.when(h != me)
             def _():
-                remote(enm.at[h], esm.at[h], sd.at[h], rd.at[h], h).wait_recv()
+                remote(enm.at[h], esm.at[h], sd.at[0], rd.at[h], h).wait_recv()
                 entry_in(0, h, se, re).wait_recv()
                 entry_in(1, h, seb, reb).wait_recv()
 
@@ -487,47 +492,13 @@
 
     for c in local[15:]:
         c.wait()
-
-    def expert_chunk(j):
-        rows_in = arrived[pl.ds(j * PER, PER)].reshape(PER * CAP, D)
-        a = jnp.dot(rows_in, gate_w[...], preferred_element_type=F32)
-        b = jnp.dot(rows_in, up_w[...], preferred_element_type=F32)
-        hidden = (a / (1.0 + jnp.exp(-a)) * b).astype(BF16)
-        made = jnp.dot(hidden, down_w[...], preferred_element_type=F32).astype(BF16)
-        produced[pl.ds(j * PER, PER)] = made.reshape(PER, CAP, D)
-
-    def expert_step(j, carry):
-        for n in range(CHUNKS):
-            @pl.when(j == n)
-            def _():
-                whole(n, outgoing, arrived, ds, dr).wait_recv()
-
-        @pl.when(j >= 1)
-        def _():
-            send_chunk(j - 1, homeward, produced, returned, bs, br)
-
-        expert_chunk(j)
-        return carry
-
-    lax.fori_loop(0, CHUNKS, expert_step, 0)
-    for j in range(CHUNKS - 1, CHUNKS):
-        send_chunk(j, homeward, produced, returned, bs, br)
-    returned[0] = produced[0]
-
-    for j in range(CHUNKS):
-        whole(j, produced, returned, bs, br).wait_recv()
-        rows_back = returned[j * PER:(j + 1) * PER].reshape(PER * CAP, D)
-        parts = jnp.dot(tab_back[:, j * C:(j + 1) * C], rows_back, preferred_element_type=F32)
-        proj[...] += parts[0:C] + parts[C:2 * C]
-    out_ref[...] = proj[...].astype(BF16)
-
-    each_peer(lambda p: remote(msg.at[p], rx1.at[me], sa.at[p], ra.at[me], p).wait_send())
-    each_peer(lambda p: remote(lsm.at[p], rxm.at[me], sc.at[p], rc.at[me], p).wait_send())
-    each_peer(lambda p: state_out(0, p, sb, rb).wait_send())
-    each_peer(lambda p: state_out(1, p, sbb, rbb).wait_send())
-    each_peer(lambda p: remote(enm.at[p], esm.at[me], sd.at[p], rd.at[me], p).wait_send())
-    each_peer(lambda p: entry_out(0, p, se, re).wait_send())
-    each_peer(lambda p: entry_out(1, p, seb, reb).wait_send())
+    fifteen(msg, rx1, sa, ra).wait_send()
+    fifteen(lsm, rxm, sc, rc).wait_send()
+    states_in(0, sb, rb).wait_send()
+    states_in(1, sbb, rbb).wait_send()
+    fifteen(enm, esm, sd, rc).wait_send()
+    states_in(0, se, rb).wait_send()
+    states_in(1, seb, rbb).wait_send()
     for n in range(6):
         to_right(dp, 0, n).wait_send()
         to_left(dp, 0, n).wait_send()
@@ -539,8 +510,43 @@
     for n in range(3):
         strip_out(n).wait_send()
         strips(n).wait_send()
+
+    def expert_chunk(j):
+        rows_in = arrived[pl.ds(j * PER, PER)].reshape(PER * CAP, D)
+        a = jnp.dot(rows_in, gate_w[...], preferred_element_type=F32)
+        b = jnp.dot(rows_in, up_w[...], preferred_element_type=F32)
+        hidden = (a / (1.0 + jnp.exp(-a)) * b).astype(BF16)
+        made = jnp.dot(hidden, down_w[...], preferred_element_type=F32).astype(BF16)
+        produced[pl.ds(j * PER, PER)] = made.reshape(PER, CAP, D)
+
+    def expert_step(j, carry):
+        for n in range(CHUNKS):
+            @pl.when(j == n)
+            def _():
+                whole(n, outgoing, arrived, ds, dr).wait_recv()
+
+        @pl.when(j >= 1)
+        def _():
+            send_chunk(j - 1, homeward, produced, returned, bs, br)
+
+        expert_chunk(j)
+        return carry
+
+    lax.fori_loop(0, CHUNKS, expert_step, 0)
+    for j in range(CHUNKS - 1, CHUNKS):
+        send_chunk(j, homeward, produced, returned, bs, br)
+    returned[0] = produced[0]
     for j in range(CHUNKS):
         whole(j, outgoing, arrived, ds, dr).wait_send()
+
+    for j in range(CHUNKS):
+        whole(j, produced, returned, bs, br).wait_recv()
+        rows_back = returned[j * PER:(j + 1) * PER].reshape(PER * CAP, D)
+        parts = jnp.dot(tab_back[:, j * C:(j + 1) * C], rows_back, preferred_element_type=F32)
+        proj[...] += parts[0:C] + parts[C:2 * C]
+    out_ref[...] = proj[...].astype(BF16)
+
+    for j in range(CHUNKS):
         whole(j, produced, returned, bs, br).wait_send()
 
 
@@ -596,7 +602,7 @@
             pltpu.VMEM((2 * C, DEVICES * CAP), BF16),
             slots, slots, slots, slots,
             dma((18,)),
-        ] + [dma((H,))] * 14 + [dma((6,))] * 4 + [dma((8,))] * 2 + [dma((3,))] * 4 + [dma((CHUNKS,))] * 4 + [pltpu.SemaphoreType.REGULAR],
+        ] + [dma((1,))] * 9 + [dma((H,)), dma((1,)), dma((H,)), dma((1,)), dma((H,))] + [dma((6,))] * 4 + [dma((8,))] * 2 + [dma((3,))] * 4 + [dma((CHUNKS,))] * 4 + [pltpu.SemaphoreType.REGULAR],
         compiler_params=pltpu.CompilerParams(
             collective_id=0, has_side_effects=True, vmem_limit_bytes=67_043_328),
         name="layer",

time: 96 us -> 93.3 us (0.972)
  Pallas kernels: 94 us -> 91.3 us
    pallas_call x1, Pallas kernels: 94 us -> 91.3 us  [on_device(): pl.pallas_call(layer_kernel, out_shape=jax.ShapeDtypeStruct((C, D), BF16)...]
where the time goes in v3:
time: 93.3 us; the launch traced here: 93.1 us
  Pallas kernels  91.3 us (98%)
  local copies, waits for them, and re-layouts  1.88 us (2%)
    pallas_call x1, Pallas kernels, on_device(): pl.pallas_call(layer_kernel, out_shape=jax.ShapeDtypeStruct((C, D), BF16)...  91.3 us
    unnamed x1, local copies, waits for them, and re-layouts  1.88 us

profile of v3, /device:TPU:1, one launch (start us, length us, event | category | flops | bytes accessed | tf_op | source)
XLA Modules:
  0.0 93.1 jit_solution(10463512781982600713)
XLA Ops:
  0.0 91.3 %layer.1 = bf16[128,2048]{1,0:T(8,128)(2,1)} custom-call(bf16[128,1024]{1,0:T(8,128)(2,1)} %bitcast.32, bf16[128,1024]{1,0:T(8,128)(2,1)} %bitcast.33, bf16[128,2048]{1,0:T(8,128)(2,1)} %bitcast.29, bf16[128,2048]{1,0:T(8,128)(2,1)} %bitcast.30, bf16[128,2048]{1,0:T(8,128)(2,1)} %bitcast.31, bf16[2048,256]{1,0:T(8,128)(2,1)} %wo_hbm.1, ...), custom_call_target="tpu_custom_call" | custom-call | tf_op jit(solution)/shard_map/layer/pallas_call | solution.py:564
  91.3 1.9 %copy.20 = bf16[1,128,2048]{2,1,0:T(8,128)(2,1)} copy(bf16[1,128,2048]{2,1,0:T(8,128)(2,1)} %bitcast.28) | data formatting | bytes 1048576

commit v4 on v3

--- a/solution.py
+++ b/solution.py
@@ -72,7 +72,7 @@
             body(peer_of(d))
             return carry
 
-        lax.fori_loop(1, H, step, 0)
+        lax.fori_loop(1, H, step, 0, unroll=True)
 
     barrier = pltpu.get_barrier_semaphore()
 

time: 93.3 us -> 92.8 us (level)
  no operation moved by 1% of the time
where the time goes in v4:
time: 92.8 us; the launch traced here: 92.6 us
  Pallas kernels  90.7 us (98%)
  local copies, waits for them, and re-layouts  1.88 us (2%)
    pallas_call x1, Pallas kernels, on_device(): pl.pallas_call(layer_kernel, out_shape=jax.ShapeDtypeStruct((C, D), BF16)...  90.7 us
    unnamed x1, local copies, waits for them, and re-layouts  1.88 us

profile of v4, /device:TPU:1, one launch (start us, length us, event | category | flops | bytes accessed | tf_op | source)
XLA Modules:
  0.0 92.6 jit_solution(9304645782001645747)
XLA Ops:
  0.0 90.7 %layer.1 = bf16[128,2048]{1,0:T(8,128)(2,1)} custom-call(bf16[128,1024]{1,0:T(8,128)(2,1)} %bitcast.32, bf16[128,1024]{1,0:T(8,128)(2,1)} %bitcast.33, bf16[128,2048]{1,0:T(8,128)(2,1)} %bitcast.29, bf16[128,2048]{1,0:T(8,128)(2,1)} %bitcast.30, bf16[128,2048]{1,0:T(8,128)(2,1)} %bitcast.31, bf16[2048,256]{1,0:T(8,128)(2,1)} %wo_hbm.1, ...), custom_call_target="tpu_custom_call" | custom-call | tf_op jit(solution)/shard_map/layer/pallas_call | solution.py:564
  90.7 1.9 %copy.20 = bf16[1,128,2048]{2,1,0:T(8,128)(2,1)} copy(bf16[1,128,2048]{2,1,0:T(8,128)(2,1)} %bitcast.28) | data formatting | bytes 1048576
